TPU v7x, 512 devices: a whole 4x4x16 slice. The times are simulated.
512 devices in a mesh: sp: 32 (over z, core), tp: 16 (over y, x).
Axes of the slice: x: 4, y: 4, z: 16, core: 2. Of those that a mesh axis runs over, the one named last changes fastest.
Arguments:
- residual: bfloat16 [4096, 2048], P('sp', 'tp'), may hold values from -48 to 48
- glu_value: bfloat16 [4096, 2048], P('sp', 'tp'), may hold values from -48 to 48
- glu_gate: bfloat16 [4096, 2048], P('sp', 'tp'), may hold values from -6 to 6
- conv_weight: bfloat16 [31, 2048], P(None, 'tp'), may hold values from -1 to 1
- conv_bias: float32 [2048], P('tp'), may hold values from -3 to 3
- ln_gain: float32 [2048], P('tp'), may hold values from 0.1 to 1.9
- ln_bias: float32 [2048], P('tp'), may hold values from -3 to 3
- out_weight: bfloat16 [2048, 2048], P(None, 'tp'), may hold values from -0.125 to 0.125
- norm_gain: float32 [2048], P('tp'), may hold values from 0.1 to 1.9
- route_ids: int32 [4096, 2], P('sp'), may hold values from 0 to 31, all different within a row; in each aligned block of 128 rows (0 to 127, 128 to 255, ...) at most 16 rows name the same one
- route_weight: float32 [4096, 2], P('sp'), may hold values from 0.1 to 1
- expert_gate: bfloat16 [32, 2048, 4096], P('sp', None, 'tp'), may hold values from -0.125 to 0.125
- expert_up: bfloat16 [32, 2048, 4096], P('sp', None, 'tp'), may hold values from -0.125 to 0.125
- expert_down: bfloat16 [32, 4096, 2048], P('sp', 'tp'), may hold values from -0.09375 to 0.09375
Outputs:
- layer_out: bfloat16 [4096, 2048], P('sp', 'tp')
Inputs may be any that keep to these rules, and one draw needn't show every extreme that they name: `route_ids`: within the 128 rows of one index of sp, no expert is named more than 16 times, and in some such rows one expert is named exactly 16 times.
All inputs are finite; a program needn't handle non-finite values.
Results may differ from a plain program's by a relative error of at most 0.006.
Values may be sent and summed in bfloat16 or wider, within the bound.
A program may use at most 64 MiB of HBM per device.

v0:
```python
import jax
import jax.numpy as jnp
from jax import lax
from jax.sharding import PartitionSpec as P

TOPK = 2


def with_halo(cells, sides, width):
    for axis, dim in sides:
        count = lax.axis_size(axis)
        ends = count - 1
        head = lax.slice_in_dim(cells, 0, width, axis=dim)
        tail = lax.slice_in_dim(cells, cells.shape[dim] - width, cells.shape[dim], axis=dim)
        cells = jnp.concatenate(
            [
                lax.ppermute(tail, axis, [(i, (i + 1) % count) for i in range(ends)]),
                cells,
                lax.ppermute(head, axis, [((i + 1) % count, i) for i in range(ends)]),
            ],
            axis=dim,
        )
    return cells


def copy_for_each(x, axis):
    copies = jnp.broadcast_to(x, (lax.axis_size(axis), *x.shape))
    return lax.all_to_all(copies, axis, split_axis=0, concat_axis=0, tiled=True)


def over_copies(x, axis):
    return copy_for_each(x, axis).sum(axis=0)


def packed_total(arrays, axis):
    vector, at, finished = (jnp.concatenate([a.reshape(-1) for a in arrays]), 0, [])
    running = over_copies(vector, axis)
    for a in arrays:
        finished.append(running[at : at + a.size].reshape(a.shape))
        at += a.size
    return tuple(finished)


def joined_along(parts, dim):
    shape = list(parts.shape[1:])
    shape[dim] *= parts.shape[0]
    return jnp.moveaxis(parts, 0, dim).reshape(shape)


def collect(x, axis, dim):
    return joined_along(copy_for_each(x, axis), dim)


def cut_along(x, dim, length):
    shape = x.shape
    parts = x.reshape(*shape[:dim], length, shape[dim] // length, *shape[dim + 1 :])
    return jnp.moveaxis(parts, dim, 0)


def sent_and_summed(x, axis, dim):
    length = lax.axis_size(axis)
    parts = lax.all_to_all(cut_along(x, dim, length), axis, 0, 0, tiled=True)
    return jnp.sum(parts.astype(jnp.float32), axis=0)


def on_device(
    residual,
    glu_value,
    glu_gate,
    conv_weight,
    conv_bias,
    ln_gain,
    ln_bias,
    out_weight,
    norm_gain,
    route_ids,
    route_weight,
    expert_gate,
    expert_up,
    expert_down,
):
    rows = residual.shape[0]
    width_all = out_weight.shape[0]
    gated = (glu_value.astype(jnp.float32) * jax.nn.sigmoid(glu_gate.astype(jnp.float32))).astype(
        jnp.bfloat16
    )
    reach = conv_weight.shape[0] // 2
    padded = with_halo(gated, (("sp", 0),), reach)
    taps = conv_weight.astype(jnp.float32)
    conv = jnp.zeros(gated.shape, jnp.float32) + conv_bias
    for tap in range(conv_weight.shape[0]):
        conv = conv + padded[tap : tap + rows].astype(jnp.float32) * taps[tap]
    totals = packed_total((jnp.sum(conv, axis=1), jnp.sum(conv * conv, axis=1)), "tp")
    mean = (totals[0] / width_all)[:, None]
    var = (totals[1] / width_all)[:, None] - mean * mean
    act = jax.nn.silu((conv - mean) * lax.rsqrt(var + 1e-05) * ln_gain + ln_bias).astype(
        jnp.bfloat16
    )
    projected = jnp.dot(collect(act, "tp", 1), out_weight, preferred_element_type=jnp.float32)
    mixed = residual.astype(jnp.float32) + projected
    squares = over_copies(jnp.sum(mixed * mixed, axis=1), "tp")
    normed = (mixed * lax.rsqrt(squares / width_all + 1e-06)[:, None] * norm_gain).astype(
        jnp.bfloat16
    )
    experts = lax.axis_size("sp")
    capacity = 2 * rows * TOPK // experts
    flat = route_ids.reshape(-1)
    onehot = (flat[:, None] == jnp.arange(experts, dtype=jnp.int32)[None, :]).astype(jnp.int32)
    rank = jnp.sum((jnp.cumsum(onehot, axis=0) - 1) * onehot, axis=1)
    slot_of = flat * capacity + rank
    placing = (slot_of[None, :] == jnp.arange(experts * capacity, dtype=jnp.int32)[:, None]).astype(
        jnp.bfloat16
    )
    copies = jnp.repeat(normed, TOPK, axis=0)
    outgoing = jnp.dot(placing, copies, preferred_element_type=jnp.float32).astype(jnp.bfloat16)
    outgoing = outgoing.reshape(experts, capacity, normed.shape[1])
    arrived = lax.all_to_all(outgoing, "sp", split_axis=0, concat_axis=0, tiled=True)
    arrived = collect(arrived.reshape(experts * capacity, normed.shape[1]), "tp", 1)
    gate = jnp.dot(arrived, expert_gate[0], preferred_element_type=jnp.float32)
    up = jnp.dot(arrived, expert_up[0], preferred_element_type=jnp.float32)
    hidden = (jax.nn.silu(gate) * up).astype(jnp.bfloat16)
    partial_out = jnp.dot(hidden, expert_down[0], preferred_element_type=jnp.float32)
    summed = sent_and_summed(partial_out.astype(jnp.bfloat16), "tp", 1).astype(jnp.bfloat16)
    summed = summed.reshape(experts, capacity, summed.shape[1])
    returned = lax.all_to_all(summed, "sp", split_axis=0, concat_axis=0, tiled=True)
    returned = returned.reshape(experts * capacity, returned.shape[2])
    picked = lax.dot_general(
        placing, returned, (((0,), (0,)), ((), ())), preferred_element_type=jnp.float32
    )
    picked = picked.reshape(rows, TOPK, picked.shape[1])
    moe = jnp.sum(picked * route_weight[:, :, None], axis=1)
    return (mixed + moe).astype(jnp.bfloat16)


def solution(mesh):
    in_specs = (
        P("sp", "tp"),
        P("sp", "tp"),
        P("sp", "tp"),
        P(None, "tp"),
        P("tp"),
        P("tp"),
        P("tp"),
        P(None, "tp"),
        P("tp"),
        P("sp", None),
        P("sp", None),
        P("sp", None, "tp"),
        P("sp", None, "tp"),
        P("sp", "tp", None),
    )
    out_specs = P("sp", "tp")
    return jax.shard_map(
        on_device, mesh=mesh, in_specs=in_specs, out_specs=out_specs, check_vma=False
    )
```

profile of v0, /device:TPU:1, one launch (start us, length us, event | category | flops | bytes accessed | tf_op | source)
XLA Modules:
  0.0 180.1 jit_solution(5758784225859526224)
XLA Ops:
  0.0 0.9 multiply_convert_fusion.2
  1.0 4.9 %collective-permute-start = (bf16[15,128]{1,0:T(8,128)(2,1)S(1)}, bf16[15,128]{1,0:T(8,128)(2,1)S(1)}, u32[]{:S(2)}, u32[]{:S(2)}) collective-permute-start(bf16[15,128]{1,0:T(8,128)(2,1)S(1)} %get-tuple-element.8), channel_id=1, source_target_pairs={{0,16},{16,32},{32,48},{48,64},{64,80},{80,96},{96,112},{112,128},... | collective-permute-start | bytes 11528 | tf_op jit(solution)/shard_map/ppermute | solution.py:17
  5.9 5.1 %collective-permute-start.1 = (bf16[15,128]{1,0:T(8,128)(2,1)S(1)}, bf16[15,128]{1,0:T(8,128)(2,1)S(1)}, u32[]{:S(2)}, u32[]{:S(2)}) collective-permute-start(bf16[15,128]{1,0:T(8,128)(2,1)S(1)} %get-tuple-element.9), channel_id=1, source_target_pairs={{16,0},{32,16},{48,32},{64,48},{80,64},{96,80},{112,96},{128,112},... | collective-permute-start | bytes 11528 | tf_op jit(solution)/shard_map/ppermute | solution.py:19
  11.0 0.7 convert_element_type.139
  11.8 1.0 fusion.51
  12.8 12.0 %all_to_all.37 = f32[16,1,256]{2,1,0:T(1,128)S(1)} all-to-all(f32[16,1,256]{2,1,0:T(1,128)S(1)} %broadcast_in_dim.10), channel_id=1, replica_groups=mesh['sp'=32,'tp'=16] {'tp'}, dimensions={0} | all-to-all | bytes 32768 | tf_op jit(solution)/shard_map/all_to_all | solution.py:28
  24.9 0.8 multiply_convert_fusion.1
  25.8 0.9 broadcast_in_dim.11
  26.7 3.6 %all-to-all-start.1 = ((bf16[16,128,128]{1,2,0:T(8,128)(2,1)}), bf16[16,128,128]{1,2,0:T(8,128)(2,1)S(1)}, u32[]{:S(2)}, u32[]{:S(2)}) async-start(bf16[16,128,128]{1,2,0:T(8,128)(2,1)} %broadcast_in_dim.11), calls=%async_computation.1 | async-start | bytes 1048576 | tf_op jit(solution)/shard_map/all_to_all | solution.py:28
  30.8 0.6 reduce-window.6
  31.8 10.9 %all-to-all-done.1 = bf16[16,128,128]{1,2,0:T(8,128)(2,1)S(1)} async-done(((bf16[16,128,128]{1,2,0:T(8,128)(2,1)}), bf16[16,128,128]{1,2,0:T(8,128)(2,1)S(1)}, u32[]{:S(2)}, u32[]{:S(2)}) %all-to-all-start.1) | async-done | bytes 524320 | tf_op jit(solution)/shard_map/all_to_all | solution.py:28
  43.0 0.6 broadcast_in_dim.12
  43.6 3.5 %all-to-all-start.2 = ((f32[16,1,128]{2,1,0:T(1,128)}), f32[16,1,128]{2,1,0:T(1,128)S(1)}, u32[]{:S(2)}, u32[]{:S(2)}) async-start(f32[16,1,128]{2,1,0:T(1,128)} %broadcast_in_dim.12), calls=%async_computation.2 | async-start | bytes 16384 | tf_op jit(solution)/shard_map/all_to_all | solution.py:28
  47.1 6.3 %all-to-all-done.2 = f32[16,1,128]{2,1,0:T(1,128)S(1)} async-done(((f32[16,1,128]{2,1,0:T(1,128)}), f32[16,1,128]{2,1,0:T(1,128)S(1)}, u32[]{:S(2)}, u32[]{:S(2)}) %all-to-all-start.2) | async-done | bytes 8224 | tf_op jit(solution)/shard_map/all_to_all | solution.py:28
  53.9 31.4 %all_to_all.38 = bf16[32,16,128]{2,1,0:T(8,128)(2,1)S(1)} all-to-all(bf16[32,16,128]{2,1,0:T(8,128)(2,1)S(1)} %bitcast.125), channel_id=1, replica_groups=mesh['sp'=32,'tp'=16] {'sp'}, dimensions={0} | all-to-all | bytes 262144 | tf_op jit(solution)/shard_map/all_to_all | solution.py:117
  85.7 29.7 %all_to_all.39 = bf16[16,512,128]{1,2,0:T(8,128)(2,1)S(1)} all-to-all(bf16[16,512,128]{1,2,0:T(8,128)(2,1)S(1)} %broadcast_in_dim.14), channel_id=1, replica_groups=mesh['sp'=32,'tp'=16] {'tp'}, dimensions={0} | all-to-all | bytes 4194304 | tf_op jit(solution)/shard_map/all_to_all | solution.py:28
  115.4 1.5 fusion.5
  117.0 5.0 %fusion = bf16[64,16,8,128]{3,2,1,0:T(8,128)(2,1)} fusion(bf16[1,256,2048]{2,1,0:T(8,128)(2,1)S(1)} %copy-done, bf16[512,2048]{0,1:T(8,128)(2,1)S(1)} %bitcast.120, bf16[1,2048,256]{2,1,0:T(8,128)(2,1)} %param.26, f32[512,256]{1,0:T(8,128)} %fusion.5), kind=kOutput, calls=%fused_computation.2 | convolution fusion | flops 1075576832 | bytes 6815744 | tf_op jit(solution)/shard_map/dot_general | solution.py:122
  122.0 2.1 %copy.90 = bf16[64,16,8,128]{3,2,0,1:T(8,128)(2,1)S(1)} copy(bf16[64,16,8,128]{3,2,1,0:T(8,128)(2,1)} %fusion) | data formatting | bytes 4194304 | tf_op jit(solution)/shard_map/reshape | solution.py:56
  124.1 28.2 %all_to_all.40 = bf16[16,512,128]{2,1,0:T(8,128)(2,1)S(1)} all-to-all(bf16[16,512,128]{2,1,0:T(8,128)(2,1)S(1)} %bitcast.121), channel_id=1, replica_groups=mesh['sp'=32,'tp'=16] {'tp'}, dimensions={0} | all-to-all | bytes 4194304 | tf_op jit(solution)/shard_map/all_to_all | solution.py:62
  152.3 0.9 reduce_sum.84
  153.3 9.8 %all-to-all-start.6 = ((bf16[32,16,128]{2,1,0:T(8,128)(2,1)}), bf16[32,16,128]{2,1,0:T(8,128)(2,1)S(1)}, u32[]{:S(2)}, u32[]{:S(2)}) async-start(bf16[32,16,128]{2,1,0:T(8,128)(2,1)} %bitcast.46), calls=%async_computation.6 | async-start | bytes 262144 | tf_op jit(solution)/shard_map/all_to_all | solution.py:125
  163.3 15.6 %all-to-all-done.6 = bf16[32,16,128]{2,1,0:T(8,128)(2,1)S(1)} async-done(((bf16[32,16,128]{2,1,0:T(8,128)(2,1)}), bf16[32,16,128]{2,1,0:T(8,128)(2,1)S(1)}, u32[]{:S(2)}, u32[]{:S(2)}) %all-to-all-start.6) | async-done | bytes 131104 | tf_op jit(solution)/shard_map/all_to_all | solution.py:125
  179.4 0.7 copy.82
  (49 shorter events, 2.9 us)
Async XLA Ops:
  0.0 117.0 %copy-start = (bf16[1,256,2048]{2,1,0:T(8,128)(2,1)S(1)}, bf16[1,256,2048]{2,1,0:T(8,128)(2,1)}, u32[]{:S(2)}) copy-start(bf16[1,256,2048]{2,1,0:T(8,128)(2,1)} %param.27) | copy-start | bytes 3145732
  0.0 30.3 %copy-start.4 = (s32[128,2]{0,1:T(2,128)S(1)}, s32[128,2]{0,1:T(2,128)}, u32[]{:S(2)}) copy-start(s32[128,2]{0,1:T(2,128)} %param.23) | copy-start | bytes 3076
  0.0 30.7 %copy-start.3 = (bf16[128,128]{1,0:T(8,128)(2,1)S(1)}, bf16[128,128]{1,0:T(8,128)(2,1)}, u32[]{:S(2)}) copy-start(bf16[128,128]{1,0:T(8,128)(2,1)} %param.14) | copy-start | bytes 98308
  0.0 42.7 %copy-start.2 = (bf16[2048,128]{1,0:T(8,128)(2,1)S(1)}, bf16[2048,128]{1,0:T(8,128)(2,1)}, u32[]{:S(2)}) copy-start(bf16[2048,128]{1,0:T(8,128)(2,1)} %param.21) | copy-start | bytes 1572868
  0.0 53.4 %copy-start.5 = (f32[128]{0:T(128)S(1)}, f32[128]{0:T(128)}, u32[]{:S(2)}) copy-start(f32[128]{0:T(128)} %param.22) | copy-start | bytes 1540
  1.0 10.8 %collective-permute-start = (bf16[15,128]{1,0:T(8,128)(2,1)S(1)}, bf16[15,128]{1,0:T(8,128)(2,1)S(1)}, u32[]{:S(2)}, u32[]{:S(2)}) collective-permute-start(bf16[15,128]{1,0:T(8,128)(2,1)S(1)} %get-tuple-element.8), channel_id=1, source_target_pairs={{0,16},{16,32},{32,48},{48,64},{64,80},{80,96},{96,112},{112,128},... | collective-permute-start | bytes 11528 | tf_op jit(solution)/shard_map/ppermute | solution.py:17
  5.9 5.9 %collective-permute-start.1 = (bf16[15,128]{1,0:T(8,128)(2,1)S(1)}, bf16[15,128]{1,0:T(8,128)(2,1)S(1)}, u32[]{:S(2)}, u32[]{:S(2)}) collective-permute-start(bf16[15,128]{1,0:T(8,128)(2,1)S(1)} %get-tuple-element.9), channel_id=1, source_target_pairs={{16,0},{32,16},{48,32},{64,48},{80,64},{96,80},{112,96},{128,112},... | collective-permute-start | bytes 11528 | tf_op jit(solution)/shard_map/ppermute | solution.py:19
  26.7 16.0 %all-to-all-start.1 = ((bf16[16,128,128]{1,2,0:T(8,128)(2,1)}), bf16[16,128,128]{1,2,0:T(8,128)(2,1)S(1)}, u32[]{:S(2)}, u32[]{:S(2)}) async-start(bf16[16,128,128]{1,2,0:T(8,128)(2,1)} %broadcast_in_dim.11), calls=%async_computation.1 | async-start | bytes 1048576 | tf_op jit(solution)/shard_map/all_to_all | solution.py:28
  43.6 9.8 %all-to-all-start.2 = ((f32[16,1,128]{2,1,0:T(1,128)}), f32[16,1,128]{2,1,0:T(1,128)S(1)}, u32[]{:S(2)}, u32[]{:S(2)}) async-start(f32[16,1,128]{2,1,0:T(1,128)} %broadcast_in_dim.12), calls=%async_computation.2 | async-start | bytes 16384 | tf_op jit(solution)/shard_map/all_to_all | solution.py:28
  85.7 29.7 %copy-start.1 = (bf16[1,2048,256]{2,1,0:T(8,128)(2,1)S(1)}, bf16[1,2048,256]{2,1,0:T(8,128)(2,1)}, u32[]{:S(2)}) copy-start(bf16[1,2048,256]{2,1,0:T(8,128)(2,1)} %param.25) | copy-start | bytes 3145732
  152.3 26.7 %copy-start.6 = (f32[128,2]{0,1:T(2,128)S(1)}, f32[128,2]{0,1:T(2,128)}, u32[]{:S(2)}) copy-start(f32[128,2]{0,1:T(2,128)} %param.24) | copy-start | bytes 3076
  153.3 25.7 %all-to-all-start.6 = ((bf16[32,16,128]{2,1,0:T(8,128)(2,1)}), bf16[32,16,128]{2,1,0:T(8,128)(2,1)S(1)}, u32[]{:S(2)}, u32[]{:S(2)}) async-start(bf16[32,16,128]{2,1,0:T(8,128)(2,1)} %bitcast.46), calls=%async_computation.6 | async-start | bytes 262144 | tf_op jit(solution)/shard_map/all_to_all | solution.py:125
where the time goes:
time: 181 us; the launch traced here: 180 us
  blocking collectives  101 us (56%)
  waiting for transfers between devices  32.9 us (18%)
  starting transfers between devices  26.9 us (15%)
  matrix products  7.46 us (4%)
  local copies, waits for them, and re-layouts  5.98 us (3%)
  other arithmetic  5.28 us (3%)
    all_to_all x2, blocking collectives, copy_for_each(): return lax.all_to_all(copies, axis, split_axis=0, concat_axis=0, tiled=True)  41.7 us
    all_to_all x1, blocking collectives, on_device(): lax.all_to_all(outgoing, 'sp', split_axis=0, concat_axis=0, tiled=True)  31.4 us
    all_to_all x1, blocking collectives, sent_and_summed(): parts = lax.all_to_all(cut_along(x, dim, length), axis, 0, 0, tiled=True)  28.2 us
    all_to_all x2, waiting for transfers between devices, copy_for_each(): return lax.all_to_all(copies, axis, split_axis=0, concat_axis=0, tiled=True)  17.2 us
    all_to_all x1, waiting for transfers between devices, on_device(): lax.all_to_all(summed, 'sp', split_axis=0, concat_axis=0, tiled=True)  15.6 us
    all_to_all x1, starting transfers between devices, on_device(): lax.all_to_all(summed, 'sp', split_axis=0, concat_axis=0, tiled=True)  9.85 us
    all_to_all x2, starting transfers between devices, copy_for_each(): return lax.all_to_all(copies, axis, split_axis=0, concat_axis=0, tiled=True)  7.04 us
    ppermute x1, starting transfers between devices, with_halo(): lax.ppermute(head, axis, [((i + 1) % count, i) for i in range(ends)])  5.11 us
  transfers between devices with their start and end apart: 5, of which 4 were waited for; matrix products, arithmetic and copies ran while one was open for 1% of the time, Pallas kernels for 0%

commit v1 on v0

v1 whole, which is shorter than its diff:
```python
import functools

import jax
import jax.numpy as jnp
from jax import lax
from jax.experimental import pallas as pl
from jax.experimental.pallas import tpu as pltpu
from jax.sharding import PartitionSpec as P

MESH = pl.DeviceIdType.MESH
TOPK = 2
F32 = jnp.float32
BF16 = jnp.bfloat16
NX = 4
CHUNKS = 2

TREE_4X4 = {
    (1, 0): (0, 0),
    (3, 0): (0, 0),
    (0, 1): (0, 0),
    (0, 3): (0, 0),
    (1, 1): (1, 0),
    (3, 1): (0, 1),
    (3, 3): (3, 0),
    (1, 3): (0, 3),
    (2, 0): (1, 0),
    (0, 2): (0, 3),
    (2, 1): (3, 1),
    (2, 3): (1, 3),
    (1, 2): (1, 1),
    (3, 2): (3, 3),
    (2, 2): (2, 1),
}


def spanning_tree(nx, ny):
    if (nx, ny) == (4, 4):
        parent = TREE_4X4
    else:
        parent, frontier = {}, [(0, 0)]
        while frontier:
            grown = []
            for px, py in frontier:
                for dx, dy in ((1, 0), (nx - 1, 0), (0, 1), (0, ny - 1)):
                    o = ((px + dx) % nx, (py + dy) % ny)
                    if o != (0, 0) and o not in parent:
                        parent[o] = (px, py)
                        grown.append(o)
            frontier = grown
    depth = {(0, 0): 0}
    order = [(0, 0)]
    for o in order:
        for c, p in parent.items():
            if p == o:
                depth[c] = depth[o] + 1
                order.append(c)
    order.sort(key=lambda o: depth[o])
    children = {o: [c for c in order if parent.get(c) == o] for o in order}
    height = {}
    for o in reversed(order):
        height[o] = 1 + max([height[c] for c in children[o]], default=-1)
    return order, parent, children, depth, height


def layer_kernel(
    ns,
    nx,
    ny,
    residual_ref,
    value_ref,
    gate_ref,
    taps_ref,
    conv_bias_ref,
    ln_gain_ref,
    ln_bias_ref,
    out_weight_hbm,
    norm_gain_ref,
    ids_ref,
    route_weight_ref,
    expert_gate_hbm,
    expert_up_hbm,
    expert_down_hbm,
    out_ref,
    out_weight,
    expert_gate,
    expert_up,
    expert_down,
    halo,
    gated,
    padded,
    stat,
    act,
    mixed,
    picks,
    places,
    outgoing,
    xbuf,
    acc_gate,
    acc_up,
    acc_sq,
    partial,
    rs_in,
    rs_out,
    ret_out,
    ret_in,
    weight_sem,
    halo_s,
    halo_r,
    stat_s,
    stat_r,
    act_s,
    act_r,
    z_s,
    z_r,
    ag_s,
    ag_r,
    rs_s,
    rs_r,
    rt_s,
    rt_r,
):
    ntp = nx * ny
    rows, width = residual_ref.shape
    total_width = ntp * width
    slots = places.shape[0]
    cap = slots // ns
    chunks = outgoing.shape[0]
    depth_rows = slots // chunks
    per_side = ns // (2 * chunks)
    taps = taps_ref.shape[0]
    reach = taps // 2
    edge = halo.shape[1]
    s = lax.axis_index("sp")
    t = lax.axis_index("tp")
    ty, tx = t // nx, lax.rem(t, nx)
    order, parent, children, depth, height = spanning_tree(nx, ny)
    number = {o: i for i, o in enumerate(order)}

    def tp_at(dx, dy):
        return lax.rem(ty + dy + 2 * ny, ny) * nx + lax.rem(tx + dx + 2 * nx, nx)

    def owner(o):
        return tp_at(-o[0], -o[1])

    def sp_at(d):
        return lax.rem(s + d + 2 * ns, ns)

    def distance(k, jj):
        return k * per_side + jj if jj < per_side else jj - (k + 2) * per_side

    def send(src, dst, send_sem, recv_sem, device):
        copy = pltpu.make_async_remote_copy(
            src_ref=src,
            dst_ref=dst,
            send_sem=send_sem,
            recv_sem=recv_sem,
            device_id=device,
            device_id_type=MESH,
        )
        copy.start()
        return copy

    barrier = pltpu.get_barrier_semaphore()
    for i in range(1, ntp):
        pl.semaphore_signal(
            barrier, inc=1, device_id=(s, lax.rem(t + i, ntp)), device_id_type=MESH
        )
    for d in range(1, ns):
        pl.semaphore_signal(barrier, inc=1, device_id=(sp_at(d), t), device_id_type=MESH)

    loads = [
        pltpu.make_async_copy(out_weight_hbm, out_weight, weight_sem.at[0]),
        pltpu.make_async_copy(expert_gate_hbm.at[0], expert_gate, weight_sem.at[1]),
        pltpu.make_async_copy(expert_up_hbm.at[0], expert_up, weight_sem.at[2]),
        pltpu.make_async_copy(expert_down_hbm.at[0], expert_down, weight_sem.at[3]),
    ]
    for load in loads:
        load.start()

    gated_f = value_ref[...].astype(F32) * jax.nn.sigmoid(gate_ref[...].astype(F32))
    gated[...] = gated_f.astype(BF16)
    padded[edge : edge + rows, :] = gated[...].astype(F32)

    expert_of = lax.broadcasted_iota(jnp.int32, (rows, ns), 1)
    chosen = [
        jnp.where(ids_ref[:, k : k + 1] == expert_of, 1.0, 0.0).astype(BF16)
        for k in range(TOPK)
    ]
    earlier = jnp.where(
        lax.broadcasted_iota(jnp.int32, (rows, rows), 1)
        < lax.broadcasted_iota(jnp.int32, (rows, rows), 0),
        1.0,
        0.0,
    ).astype(BF16)
    rank = jnp.dot(earlier, chosen[0] + chosen[1], preferred_element_type=F32).astype(BF16)
    slot = lax.broadcasted_iota(jnp.int32, (ns, slots), 1)
    in_chunk = (slot // cap) & (2 * per_side - 1)
    chunk_of = slot // depth_rows
    away = in_chunk + chunk_of * per_side
    away = jnp.where(in_chunk >= per_side, away - (2 * chunk_of + 2) * per_side, away)
    spread = jnp.where(
        lax.broadcasted_iota(jnp.int32, (ns, slots), 0) == ((s + away + 2 * ns) & (ns - 1)),
        1.0,
        0.0,
    ).astype(BF16)
    rank_at = jnp.dot(rank, spread, preferred_element_type=F32)
    slot_rank = (lax.broadcasted_iota(jnp.int32, (rows, slots), 1) & (cap - 1)).astype(F32)
    hit = rank_at == slot_rank
    both = jnp.zeros((rows, slots), F32)
    for k in range(TOPK):
        here = jnp.dot(chosen[k], spread, preferred_element_type=F32)
        here = jnp.where(hit, here, 0.0)
        picks[k] = here.astype(BF16)
        both = both + here
    places[...] = both.T.astype(BF16)

    ln_gain_col = jnp.broadcast_to(ln_gain_ref[...], (rows, width)).T
    ln_bias_col = jnp.broadcast_to(ln_bias_ref[...], (rows, width)).T

    pl.semaphore_wait(barrier, ntp - 1 + ns - 1)

    to_right = send(
        gated.at[pl.ds(rows - edge, edge)], halo.at[0], halo_s.at[0], halo_r.at[0], (sp_at(1), t)
    )
    to_left = send(gated.at[pl.ds(0, edge)], halo.at[1], halo_s.at[1], halo_r.at[1], (sp_at(-1), t))
    pending = [to_right, to_left]
    to_right.wait_recv()
    to_left.wait_recv()
    padded[0:edge, :] = jnp.where(s > 0, halo[0].astype(F32), 0.0)
    padded[edge + rows : edge + rows + edge, :] = jnp.where(
        s < ns - 1, halo[1].astype(F32), 0.0
    )
    tap_values = taps_ref[...].astype(F32)
    conv = jnp.zeros((rows, width), F32) + conv_bias_ref[...]
    for tap in range(taps):
        start = edge - reach + tap
        conv = conv + padded[start : start + rows, :] * tap_values[tap : tap + 1, :]
    conv_t = conv.T
    stat_row = jnp.concatenate(
        [
            jnp.sum(conv_t, axis=0, keepdims=True),
            jnp.sum(conv_t * conv_t, axis=0, keepdims=True),
            1.0 / norm_gain_ref[...],
            jnp.zeros((5, width), F32),
        ],
        axis=0,
    )
    stat[t] = stat_row
    arriving = []
    for i in range(1, ntp):
        arriving.append(
            send(
                stat.at[t],
                stat.at[t],
                stat_s.at[i],
                stat_r.at[i],
                (s, lax.rem(t + i, ntp)),
            )
        )
    for copy in arriving:
        copy.wait_recv()
    pending += arriving
    totals = jnp.sum(stat[...], axis=0) * (1.0 / total_width)
    mean = totals[0:1, :]
    var = totals[1:2, :] - mean * mean
    scaled = (conv_t - mean) * lax.rsqrt(var + 1e-05) * ln_gain_col + ln_bias_col
    act[t] = jax.nn.silu(scaled).T.astype(BF16)
    arriving = []
    for i in range(1, ntp):
        arriving.append(
            send(act.at[t], act.at[t], act_s.at[i], act_r.at[i], (s, lax.rem(t + i, ntp)))
        )
    loads[0].wait()
    for copy in arriving:
        copy.wait_recv()
    pending += arriving
    all_act = jnp.concatenate([act[i] for i in range(ntp)], axis=1)
    projected = jnp.dot(all_act, out_weight[...], preferred_element_type=F32)
    total = residual_ref[...].astype(F32) + projected
    mixed[...] = total
    scaled_rows = (total * norm_gain_ref[...]).astype(BF16)

    dispatch = {}
    for k in range(chunks):
        outgoing[k] = jnp.dot(
            places[k * depth_rows : (k + 1) * depth_rows, :],
            scaled_rows,
            preferred_element_type=F32,
        ).astype(BF16)
        for jj in range(2 * per_side):
            d = distance(k, jj)
            part = pl.ds(jj * cap, cap)
            if d == 0:
                xbuf[k, 0, part, :] = outgoing[k, part, :]
            else:
                dispatch[k, jj] = send(
                    outgoing.at[k, part],
                    xbuf.at[k, 0, part],
                    z_s.at[k, jj],
                    z_r.at[k, jj],
                    (sp_at(d), t),
                )
    pending += list(dispatch.values())
    for load in loads[1:]:
        load.wait()

    gathers, sums, returns = {}, {}, {}

    def pass_on(k, o):
        if o == (0, 0):
            for (kk, _), copy in dispatch.items():
                if kk == k:
                    copy.wait_recv()
        else:
            gathers[k, o].wait_recv()
        for c in children[o]:
            gathers[k, c] = send(
                xbuf.at[k, number[o]],
                xbuf.at[k, number[c]],
                ag_s.at[k, number[c]],
                ag_r.at[k, number[c]],
                (s, tp_at(c[0] - o[0], c[1] - o[1])),
            )

    def multiply(k, group, first):
        blocks = [xbuf[k, number[o]] for o in group]
        owners = [owner(o) for o in group]
        wide = jnp.concatenate(blocks, axis=1)
        squares = None if first else acc_sq[k]
        for block, who in zip(blocks, owners):
            plain = block.astype(F32) * stat[who, 2:3, :]
            squares = plain * plain if squares is None else squares + plain * plain
        acc_sq[k] = squares
        for weight, acc in ((expert_gate, acc_gate), (expert_up, acc_up)):
            tall = jnp.concatenate(
                [weight[pl.ds(pl.multiple_of(who * width, width), width), :] for who in owners],
                axis=0,
            )
            product = jnp.dot(wide, tall, preferred_element_type=F32)
            acc[k] = product if first else acc[k] + product

    def finish_rows(k):
        square = jnp.sum(acc_sq[k], axis=1, keepdims=True) * (1.0 / total_width)
        scale = lax.rsqrt(square + 1e-06)
        hidden = (jax.nn.silu(acc_gate[k] * scale) * (acc_up[k] * scale)).astype(BF16)
        for i in range(ntp):
            partial[k, i] = jnp.dot(
                hidden, expert_down[:, i * width : (i + 1) * width], preferred_element_type=F32
            ).astype(BF16)

    def sum_up(k, o):
        who = owner(o)
        source = partial.at[k, who]
        if children[o]:
            value = partial[k, who].astype(F32)
            for c in children[o]:
                sums[k, c].wait_recv()
                value = value + rs_in[k, number[c]].astype(F32)
            if o == (0, 0):
                ret_out[k] = value.astype(BF16)
                return
            rs_out[k, number[o]] = value.astype(BF16)
            source = rs_out.at[k, number[o]]
        p = parent[o]
        sums[k, o] = send(
            source,
            rs_in.at[k, number[o]],
            rs_s.at[k, number[o]],
            rs_r.at[k, number[o]],
            (s, tp_at(p[0] - o[0], p[1] - o[1])),
        )

    def give_back(k):
        for jj in range(2 * per_side):
            d = distance(k, jj)
            part = pl.ds(jj * cap, cap)
            if d == 0:
                ret_in[k, part, :] = ret_out[k, part, :]
            else:
                returns[k, jj] = send(
                    ret_out.at[k, part],
                    ret_in.at[k, part],
                    rt_s.at[k, jj],
                    rt_r.at[k, jj],
                    (sp_at(-d), t),
                )

    levels = max(depth.values())
    heights = max(height.values())
    split = max(1, levels // 2)
    events = []
    for k in range(chunks):
        base = 2.0 * k
        for level in range(levels + 1):
            at = [o for o in order if depth[o] == level]
            events.append((base + level, [functools.partial(pass_on, k, o) for o in at]))
        groups = [
            [o for o in order if depth[o] <= 1],
            [o for o in order if depth[o] == 2],
            [o for o in order if depth[o] > 2],
        ]
        for i, group in enumerate(groups):
            if group:
                when = base + max(depth[o] for o in group) + 0.5
                events.append((when, [functools.partial(multiply, k, group, i == 0)]))
        events.append((base + levels + 0.6, [functools.partial(finish_rows, k)]))
        for h in range(heights + 1):
            at = [o for o in order if height[o] == h]
            at.sort(key=lambda o: -depth[o])
            events.append(
                (base + levels + 0.7 + 1.2 * h, [functools.partial(sum_up, k, o) for o in at])
            )
        events.append(
            (base + levels + 0.8 + 1.2 * heights, [functools.partial(give_back, k)])
        )
    events.sort(key=lambda e: e[0])
    for _, steps in events:
        for step in steps:
            step()

    for copy in returns.values():
        copy.wait_recv()
    answer = jnp.concatenate([ret_in[k] for k in range(chunks)], axis=0)
    result = mixed[...]
    for k in range(TOPK):
        picked = jnp.dot(picks[k], answer, preferred_element_type=F32)
        result = result + picked * route_weight_ref[:, k : k + 1]
    out_ref[...] = result.astype(BF16)

    pending += list(gathers.values()) + list(sums.values()) + list(returns.values())
    for copy in pending:
        copy.wait_send()


def on_device(ns, nx, ny, *args):
    (
        residual,
        glu_value,
        glu_gate,
        conv_weight,
        conv_bias,
        ln_gain,
        ln_bias,
        out_weight,
        norm_gain,
        route_ids,
        route_weight,
        expert_gate,
        expert_up,
        expert_down,
    ) = args
    ntp = nx * ny
    rows, width = residual.shape
    hidden = expert_gate.shape[2]
    capacity = 2 * rows * TOPK // ns
    slots = ns * capacity
    k, rc = CHUNKS, slots // CHUNKS
    edge = 16
    row = lambda v: v.reshape(1, -1)
    vmem = pl.BlockSpec(memory_space=pltpu.VMEM)
    hbm = pl.BlockSpec(memory_space=pltpu.HBM)
    dma = pltpu.SemaphoreType.DMA
    return pl.pallas_call(
        functools.partial(layer_kernel, ns, nx, ny),
        out_shape=jax.ShapeDtypeStruct(residual.shape, BF16),
        in_specs=[vmem] * 7 + [hbm] + [vmem] * 3 + [hbm] * 3,
        out_specs=vmem,
        scratch_shapes=[
            pltpu.VMEM(out_weight.shape, BF16),
            pltpu.VMEM(expert_gate.shape[1:], BF16),
            pltpu.VMEM(expert_up.shape[1:], BF16),
            pltpu.VMEM(expert_down.shape[1:], BF16),
            pltpu.VMEM((2, edge, width), BF16),
            pltpu.VMEM((rows, width), BF16),
            pltpu.VMEM((rows + 2 * edge, width), F32),
            pltpu.VMEM((ntp, 8, width), F32),
            pltpu.VMEM((ntp, rows, width), BF16),
            pltpu.VMEM((rows, width), F32),
            pltpu.VMEM((TOPK, rows, slots), BF16),
            pltpu.VMEM((slots, rows), BF16),
            pltpu.VMEM((k, rc, width), BF16),
            pltpu.VMEM((k, ntp, rc, width), BF16),
            pltpu.VMEM((k, rc, hidden), F32),
            pltpu.VMEM((k, rc, hidden), F32),
            pltpu.VMEM((k, rc, width), F32),
            pltpu.VMEM((k, ntp, rc, width), BF16),
            pltpu.VMEM((k, ntp, rc, width), BF16),
            pltpu.VMEM((k, ntp, rc, width), BF16),
            pltpu.VMEM((k, rc, width), BF16),
            pltpu.VMEM((k, rc, width), BF16),
            dma((4,)),
            dma((2,)),
            dma((2,)),
            dma((ntp,)),
            dma((ntp,)),
            dma((ntp,)),
            dma((ntp,)),
            dma((k, ns // k)),
            dma((k, ns // k)),
            dma((k, ntp)),
            dma((k, ntp)),
            dma((k, ntp)),
            dma((k, ntp)),
            dma((k, ns // k)),
            dma((k, ns // k)),
        ],
        compiler_params=pltpu.CompilerParams(
            collective_id=0, has_side_effects=True, vmem_limit_bytes=48 * 1024 * 1024
        ),
        name="layer",
    )(
        residual,
        glu_value,
        glu_gate,
        conv_weight,
        row(conv_bias),
        row(ln_gain),
        row(ln_bias),
        out_weight,
        row(norm_gain),
        route_ids,
        route_weight,
        expert_gate,
        expert_up,
        expert_down,
    )


IN_SPECS = (
    P("sp", "tp"),
    P("sp", "tp"),
    P("sp", "tp"),
    P(None, "tp"),
    P("tp"),
    P("tp"),
    P("tp"),
    P(None, "tp"),
    P("tp"),
    P("sp", None),
    P("sp", None),
    P("sp", None, "tp"),
    P("sp", None, "tp"),
    P("sp", "tp", None),
)


def solution(mesh, nx=NX):
    ns, ntp = mesh.shape["sp"], mesh.shape["tp"]
    return jax.shard_map(
        functools.partial(on_device, ns, nx, ntp // nx),
        mesh=mesh,
        in_specs=IN_SPECS,
        out_specs=P("sp", "tp"),
        check_vma=False,
    )
```

time: 181 us -> 100 us (0.55)
  blocking collectives: 101 us -> 0 us
  Pallas kernels: 0 us -> 92.1 us
  waiting for transfers between devices: 32.9 us -> 0 us
  starting transfers between devices: 26.9 us -> 0 us
  matrix products: 7.46 us -> 0 us
  other arithmetic: 5.28 us -> 0 us
    all_to_all x4 -> x0, blocking collectives: 101 us -> none  [the longest x2 41.7 us: copy_for_each(): return lax.all_to_all(copies, axis, split_axis=0, concat_axis=0, tiled=True)]
    pallas_call x0 -> x1, Pallas kernels: none -> 92.1 us  [on_device(): pl.pallas_call(functools.partial(layer_kernel, ns, nx, ny), out_shape=jax...]
    all_to_all x3 -> x0, waiting for transfers between devices: 32.8 us -> none  [the longest x2 17.2 us: copy_for_each(): return lax.all_to_all(copies, axis, split_axis=0, concat_axis=0, tiled=True)]
    all_to_all x3 -> x0, starting transfers between devices: 16.9 us -> none  [the longest x1 9.85 us: on_device(): lax.all_to_all(summed, 'sp', split_axis=0, concat_axis=0, tiled=True)]
    ppermute x2 -> x0, starting transfers between devices: 10 us -> none  [the longest x1 5.11 us: with_halo(): lax.ppermute(head, axis, [((i + 1) % count, i) for i in range(ends)])]
    dot_general x5 -> x0, matrix products: 7.46 us -> none  [the longest x1 5.04 us: on_device(): jnp.dot(hidden, expert_down[0], preferred_element_type=jnp.float32)]
    unnamed x16 -> x31, local copies, waits for them, and re-layouts: 0.25 us -> 7.43 us
    convert_element_type x6 -> x0, other arithmetic: 2.51 us -> none  [the longest x1 0.92 us: on_device(): (glu_value.astype(jnp.float32) * jax.nn.sigmoid(glu_gate.astype(jnp.float...]
  transfers between devices with their start and end apart: 5 -> 0, of which waited for: 4 -> 0; matrix products, arithmetic and copies ran while one was open for 1% -> 0% of each run, Pallas kernels for 0% -> 0%
where the time goes in v1:
time: 100 us; the launch traced here: 99.6 us
  Pallas kernels  92.1 us (92%)
  local copies, waits for them, and re-layouts  7.43 us (7%)
    pallas_call x1, Pallas kernels, on_device(): pl.pallas_call(functools.partial(layer_kernel, ns, nx, ny), out_shape=jax...  92.1 us
    unnamed x31, local copies, waits for them, and re-layouts  7.43 us

profile of v1, /device:TPU:1, one launch (start us, length us, event | category | flops | bytes accessed | tf_op | source)
XLA Modules:
  0.0 99.6 jit_solution(18082838905373068793)
XLA Ops:
  0.0 0.0 copy-start.12
  0.0 0.7 copy-done.12
  0.7 0.0 copy-start.13
  0.7 0.0 copy-start.6
  0.7 0.0 copy-start.7
  0.7 0.0 copy-start.10
  0.7 0.0 copy-start.11
  0.7 0.1 copy.15.ids_ref
  0.8 0.5 copy-done.13
  1.4 0.1 copy.16.route_weight_ref
  1.5 0.0 copy-done.6
  1.5 0.0 copy-done.7
  1.5 0.0 copy-done.10
  1.5 0.0 copy-done.11
  1.5 0.6 copy-done.4
  2.1 0.0 copy-done.5
  2.1 0.0 copy-done.8
  2.1 0.0 copy-done.9
  2.1 1.2 %copy-done = bf16[1,2048,256]{2,1,0:T(8,128)(2,1)S(1)} copy-done((bf16[1,2048,256]{2,1,0:T(8,128)(2,1)S(1)}, bf16[1,2048,256]{2,1,0:T(8,128)(2,1)}, u32[]{:S(2)}) %copy-start) | copy-done | bytes 1048600
  3.4 1.2 %copy-done.1 = bf16[1,2048,256]{2,1,0:T(8,128)(2,1)S(1)} copy-done((bf16[1,2048,256]{2,1,0:T(8,128)(2,1)S(1)}, bf16[1,2048,256]{2,1,0:T(8,128)(2,1)}, u32[]{:S(2)}) %copy-start.1) | copy-done | bytes 1048600
  4.6 1.2 %copy-done.2 = bf16[1,256,2048]{2,1,0:T(8,128)(2,1)S(1)} copy-done((bf16[1,256,2048]{2,1,0:T(8,128)(2,1)S(1)}, bf16[1,256,2048]{2,1,0:T(8,128)(2,1)}, u32[]{:S(2)}) %copy-start.2) | copy-done | bytes 1048600
  5.8 1.0 %copy-done.3 = bf16[2048,128]{1,0:T(8,128)(2,1)S(1)} copy-done((bf16[2048,128]{1,0:T(8,128)(2,1)S(1)}, bf16[2048,128]{1,0:T(8,128)(2,1)}, u32[]{:S(2)}) %copy-start.3) | copy-done | bytes 524312
  6.9 92.1 %layer.1 = bf16[128,128]{1,0:T(8,128)(2,1)S(1)} custom-call(bf16[128,128]{1,0:T(8,128)(2,1)S(1)} %copy-done.4, bf16[128,128]{1,0:T(8,128)(2,1)S(1)} %copy-done.5, bf16[128,128]{1,0:T(8,128)(2,1)S(1)} %copy-done.6, bf16[31,128]{1,0:T(8,128)(2,1)S(1)} %copy-done.7, f32[1,128]{1,0:T(1,128)S(1)} %bitcast.4, f32[1,128]{1,0:T(1,128)S(1)} %bitcast.5, ...), custom_call_target="tpu_custom_call" | custom-call | tf_op jit(solution)/shard_map/layer/pallas_call | solution.py:463
  98.9 0.6 copy.18
  (8 shorter events, 0.0 us)
Async XLA Ops:
  0.0 0.7 copy-start.12
  0.7 0.7 copy-start.13
  0.7 0.8 copy-start.6
  0.7 0.8 copy-start.7
  0.7 0.8 copy-start.10
  0.7 0.8 copy-start.11
  1.4 0.8 copy-start.4
  1.4 0.8 copy-start.5
  1.4 0.8 copy-start.8
  1.4 0.8 copy-start.9
  2.1 1.2 %copy-start = (bf16[1,2048,256]{2,1,0:T(8,128)(2,1)S(1)}, bf16[1,2048,256]{2,1,0:T(8,128)(2,1)}, u32[]{:S(2)}) copy-start(bf16[1,2048,256]{2,1,0:T(8,128)(2,1)} %expert_gate_hbm.1) | copy-start | bytes 3145732
  3.4 1.2 %copy-start.1 = (bf16[1,2048,256]{2,1,0:T(8,128)(2,1)S(1)}, bf16[1,2048,256]{2,1,0:T(8,128)(2,1)}, u32[]{:S(2)}) copy-start(bf16[1,2048,256]{2,1,0:T(8,128)(2,1)} %expert_up_hbm.1) | copy-start | bytes 3145732
  4.6 1.2 %copy-start.2 = (bf16[1,256,2048]{2,1,0:T(8,128)(2,1)S(1)}, bf16[1,256,2048]{2,1,0:T(8,128)(2,1)}, u32[]{:S(2)}) copy-start(bf16[1,256,2048]{2,1,0:T(8,128)(2,1)} %expert_down_hbm.1) | copy-start | bytes 3145732
  5.8 1.0 %copy-start.3 = (bf16[2048,128]{1,0:T(8,128)(2,1)S(1)}, bf16[2048,128]{1,0:T(8,128)(2,1)}, u32[]{:S(2)}) copy-start(bf16[2048,128]{1,0:T(8,128)(2,1)} %out_weight_hbm.1) | copy-start | bytes 1572868

commit v2 on v1

v2 whole, which is shorter than its diff:
```python
import functools

import jax
import jax.numpy as jnp
from jax import lax
from jax.experimental import pallas as pl
from jax.experimental.pallas import tpu as pltpu
from jax.sharding import PartitionSpec as P

MESH = pl.DeviceIdType.MESH
TOPK = 2
F32 = jnp.float32
BF16 = jnp.bfloat16
NX = 4
CHUNKS = 4
SEND_ORDER = (0, 2, 3, 1)
URGENCY = (1, 0, 2, 3)
KINDS = (0, 0, 0, 1)

TREE_4X4 = {
    (1, 0): (0, 0),
    (3, 0): (0, 0),
    (0, 1): (0, 0),
    (0, 3): (0, 0),
    (1, 1): (1, 0),
    (3, 1): (0, 1),
    (3, 3): (3, 0),
    (1, 3): (0, 3),
    (2, 0): (1, 0),
    (0, 2): (0, 3),
    (2, 1): (3, 1),
    (2, 3): (1, 3),
    (1, 2): (1, 1),
    (3, 2): (3, 3),
    (2, 2): (2, 1),
}
SHALLOW_4X4 = {
    **{o: (0, 0) for o in TREE_4X4},
    (2, 0): (1, 0),
    (0, 2): (0, 3),
    (2, 1): (1, 1),
    (2, 3): (3, 3),
    (1, 2): (1, 3),
    (3, 2): (3, 1),
    (2, 2): (1, 1),
}


def turned(tree, quarters):
    def turn(o):
        for _ in range(quarters):
            o = (-o[1] % 4, o[0])
        return o

    return {turn(c): turn(p) for c, p in tree.items()}


class Tree:
    def __init__(self, nx, ny, kind, quarters):
        if (nx, ny) == (4, 4):
            parent = turned(SHALLOW_4X4 if kind else TREE_4X4, quarters)
        else:
            parent, frontier = {}, [(0, 0)]
            while frontier:
                grown = []
                for px, py in frontier:
                    for dx, dy in ((1, 0), (nx - 1, 0), (0, 1), (0, ny - 1)):
                        o = ((px + dx) % nx, (py + dy) % ny)
                        if o != (0, 0) and o not in parent:
                            parent[o] = (px, py)
                            grown.append(o)
                frontier = grown
        self.parent = parent
        self.depth = {(0, 0): 0}
        self.order = [(0, 0)]
        for o in self.order:
            for c in sorted(parent):
                if parent[c] == o:
                    self.depth[c] = self.depth[o] + 1
                    self.order.append(c)
        self.children = {o: [c for c in self.order if parent.get(c) == o] for o in self.order}
        self.groups = [
            [o for o in self.order if low <= self.depth[o] <= high]
            for low, high in ((0, 1), (2, 2), (3, 9))
        ]
        self.groups = [g for g in self.groups if g]


def signed(v, n):
    return (v + n // 2 - 1) % n - (n // 2 - 1)


def plan(trees, nx, ny, rows, arrivals, urgency):
    wire, latency, hop = rows * 256 / 46.65e3, 2.2, 0.75
    link, now, steps, pending = {}, 0.0, [], []
    arrived, summed, passed, given = {}, {}, {}, {}

    def sent(p, o):
        dx, dy = signed(o[0] - p[0], nx), signed(o[1] - p[1], ny)
        end = now
        for axis, v, n in ((0, dx, nx), (1, dy, ny)):
            if v:
                for way in (1, -1) if 2 * v == n else (1 if v > 0 else -1,):
                    link[axis, way] = max(link.get((axis, way), 0.0), now) + wire
                    end = max(end, link[axis, way])
        return end + latency + hop * (abs(dx) + abs(dy) - 1)

    for k in range(len(trees)):
        pending.append(("pass", k, (0, 0)))
        passed[k], given[k] = set(), 0
    finished = 0
    while finished < len(trees):
        ready = {}
        for e in pending:
            kind, k, o = e
            if kind == "pass":
                ready[e] = arrived[k, o] if o != (0, 0) else arrivals[k]
            elif kind == "sum":
                ready[e] = max([summed[k, c] for c in trees[k].children[o]], default=0.0)
            else:
                ready[e] = 0.0

        def rank(e):
            kind, k, o = e
            late = -trees[k].depth[o] if kind == "sum" else 0
            return ({"pass": 0, "sum": 0, "finish": 1}.get(kind, 2), urgency[k], late, str(o))

        able = [e for e in pending if ready[e] <= now + 1e-9]
        if able:
            e = min(able, key=rank)
        else:
            e = min(pending, key=lambda e: (ready[e], rank(e)))
        pending.remove(e)
        now = max(now, ready[e])
        steps.append(e)
        kind, k, o = e
        tree = trees[k]
        if kind == "pass":
            for c in tree.children[o]:
                arrived[k, c] = sent(o, c)
                pending.append(("pass", k, c))
            now += 0.03
            passed[k].add(o)
            while given[k] < len(tree.groups) and passed[k].issuperset(tree.groups[given[k]]):
                pending.append(("multiply", k, given[k]))
                given[k] += 1
        elif kind == "multiply":
            now += 0.15
            if given[k] == len(tree.groups) and not any(e[:2] == (kind, k) for e in pending):
                pending.append(("finish", k, 0))
        elif kind == "finish":
            now += 0.5
            pending += [("sum", k, c) for c in tree.order if not tree.children[c]]
        else:
            now += 0.05 if tree.children[o] else 0.02
            if o == (0, 0):
                finished += 1
            else:
                p = tree.parent[o]
                summed[k, o] = sent(o, p)
                if all((k, c) in summed for c in tree.children[p]):
                    pending.append(("sum", k, p))
    return steps


def layer_kernel(
    ns,
    nx,
    ny,
    *refs,
):
    sources, (out_ref, *scratch) = refs[:14], refs[14:]
    (
        residual_ref,
        value_ref,
        gate_ref,
        taps_ref,
        conv_bias_ref,
        ln_gain_ref,
        ln_bias_ref,
        out_weight,
        norm_gain_ref,
        ids_ref,
        route_weight_ref,
        expert_gate,
        expert_up,
        expert_down,
    ) = scratch[:14]
    (
        halo,
        gated,
        padded,
        stat,
        act,
        mixed,
        picks,
        places,
        route_cols,
        outgoing,
        xbuf,
        acc_gate,
        acc_up,
        acc_sq,
        partial,
        rs_in,
        rs_out,
        ret_out,
        ret_in,
        met,
        load_sem,
        halo_s,
        halo_r,
        stat_s,
        stat_r,
        act_s,
        act_r,
        z_s,
        z_r,
        ag_s,
        ag_r,
        rs_s,
        rs_r,
        rt_s,
        rt_r,
    ) = scratch[14:]
    ntp = nx * ny
    rows, width = residual_ref.shape
    total_width = ntp * width
    slots = places.shape[0]
    cap = slots // ns
    chunks = outgoing.shape[0]
    depth_rows = slots // chunks
    per_side = ns // (2 * chunks)
    taps = taps_ref.shape[0]
    reach = taps // 2
    edge = halo.shape[1]
    s = lax.axis_index("sp")
    t = lax.axis_index("tp")
    ty, tx = t // nx, lax.rem(t, nx)
    trees = [Tree(nx, ny, KINDS[k], k) for k in range(chunks)]
    offsets = sorted(trees[0].order, key=lambda o: (abs(signed(o[0], nx)) + abs(signed(o[1], ny)), o))
    number = {o: i for i, o in enumerate(offsets)}

    def tp_at(dx, dy):
        return lax.rem(ty + dy + 2 * ny, ny) * nx + lax.rem(tx + dx + 2 * nx, nx)

    def owner(o):
        return tp_at(-o[0], -o[1])

    def sp_at(d):
        return lax.rem(s + d + 2 * ns, ns)

    def distance(k, jj):
        return k * per_side + jj if jj < per_side else jj - (k + 2) * per_side

    def meet(r):
        if r > 0 and 2 ** (r - 1) < ns // 2:
            pl.semaphore_wait(met.at[r - 1], 2)
        if 2**r < ns // 2:
            for d in (2**r, -(2**r)):
                pl.semaphore_signal(
                    met.at[r], inc=1, device_id=(sp_at(d), t), device_id_type=MESH
                )

    def send(src, dst, send_sem, recv_sem, device):
        copy = pltpu.make_async_remote_copy(
            src_ref=src,
            dst_ref=dst,
            send_sem=send_sem,
            recv_sem=recv_sem,
            device_id=device,
            device_id_type=MESH,
        )
        copy.start()
        return copy

    with jax.named_scope("signal"):
        barrier = pltpu.get_barrier_semaphore()
        for i in range(1, ntp):
            pl.semaphore_signal(
                barrier, inc=1, device_id=(s, lax.rem(t + i, ntp)), device_id_type=MESH
            )
        for d in (1, -1):
            pl.semaphore_signal(barrier, inc=1, device_id=(sp_at(d), t), device_id_type=MESH)

        loads = {}
        for i in (1, 2, 9, 3, 4, 5, 6, 8, 10, 0, 7, 11, 12, 13):
            source = sources[i].at[0] if i >= 11 else sources[i]
            loads[i] = pltpu.make_async_copy(source, scratch[i], load_sem.at[i])
        for load in loads.values():
            load.start()

    with jax.named_scope("local"):
        loads[1].wait()
        loads[2].wait()
        gated_f = value_ref[...].astype(F32) * jax.nn.sigmoid(gate_ref[...].astype(F32))
        gated[...] = gated_f.astype(BF16)
        padded[edge : edge + rows, :] = gated[...].astype(F32)

        for i in (9, 3, 4, 5, 6, 8, 10, 0):
            loads[i].wait()
        expert_of = lax.broadcasted_iota(jnp.int32, (ns, rows), 0)
        chosen = [
            jnp.where(ids_ref[k : k + 1, :] == expert_of, 1.0, 0.0).astype(BF16)
            for k in range(TOPK)
        ]
        earlier = jnp.where(
            lax.broadcasted_iota(jnp.int32, (rows, rows), 0)
            < lax.broadcasted_iota(jnp.int32, (rows, rows), 1),
            1.0,
            0.0,
        ).astype(BF16)
        rank = jnp.dot(chosen[0] + chosen[1], earlier, preferred_element_type=F32).astype(BF16)
        slot = lax.broadcasted_iota(jnp.int32, (slots, ns), 0)
        in_chunk = (slot // cap) & (2 * per_side - 1)
        chunk_of = slot // depth_rows
        away = in_chunk + chunk_of * per_side
        away = jnp.where(in_chunk >= per_side, away - (2 * chunk_of + 2) * per_side, away)
        spread = jnp.where(
            lax.broadcasted_iota(jnp.int32, (slots, ns), 1) == ((s + away + 2 * ns) & (ns - 1)),
            1.0,
            0.0,
        ).astype(BF16)
        rank_at = jnp.dot(spread, rank, preferred_element_type=F32)
        slot_rank = (lax.broadcasted_iota(jnp.int32, (slots, rows), 0) & (cap - 1)).astype(F32)
        hit = rank_at == slot_rank
        both = jnp.zeros((slots, rows), F32)
        for k in range(TOPK):
            here = jnp.dot(spread, chosen[k], preferred_element_type=F32)
            here = jnp.where(hit, here, 0.0)
            picks[k] = here.T.astype(BF16)
            both = both + here
            route_cols[k] = jnp.broadcast_to(route_weight_ref[k : k + 1, :], (width, rows)).T
        places[...] = both.astype(BF16)

    with jax.named_scope("barrier"):
        pl.semaphore_wait(barrier, ntp - 1 + 2)
        meet(0)

    with jax.named_scope("halo"):
        to_right = send(
            gated.at[pl.ds(rows - edge, edge)], halo.at[0], halo_s.at[0], halo_r.at[0], (sp_at(1), t)
        )
        to_left = send(gated.at[pl.ds(0, edge)], halo.at[1], halo_s.at[1], halo_r.at[1], (sp_at(-1), t))
        pending = [to_right, to_left]
        meet(1)
        to_right.wait_recv()
        to_left.wait_recv()
        meet(2)
        padded[0:edge, :] = jnp.where(s > 0, halo[0].astype(F32), 0.0)
        padded[edge + rows : edge + rows + edge, :] = jnp.where(
            s < ns - 1, halo[1].astype(F32), 0.0
        )
    with jax.named_scope("conv"):
        tap_values = taps_ref[...].astype(F32)
        conv = jnp.zeros((rows, width), F32) + conv_bias_ref[...]
        for tap in range(taps):
            start = edge - reach + tap
            conv = conv + padded[start : start + rows, :] * tap_values[tap : tap + 1, :]
        conv_t = conv.T
        stat[t] = jnp.concatenate(
            [
                jnp.sum(conv_t, axis=0, keepdims=True),
                jnp.sum(conv_t * conv_t, axis=0, keepdims=True),
                1.0 / norm_gain_ref[...],
                ln_gain_ref[...],
                ln_bias_ref[...],
                jnp.zeros((3, width), F32),
            ],
            axis=0,
        )
        stat_copies = []
        for o in reversed(offsets[1:]):
            i = number[o]
            stat_copies.append(
                send(stat.at[t], stat.at[t], stat_s.at[i], stat_r.at[i], (s, tp_at(*o)))
            )
        own_mean = jnp.sum(conv, axis=1, keepdims=True) * (1.0 / width)
        act[0] = (conv - own_mean).astype(BF16)
        act_copies = {}
        for o in reversed(offsets[1:]):
            i = number[o]
            act_copies[o] = send(
                act.at[0], act.at[i], act_s.at[i], act_r.at[i], (s, tp_at(*o))
            )
    with jax.named_scope("stats"):
        meet(3)
        for copy in stat_copies:
            copy.wait_recv()
        pending += stat_copies + list(act_copies.values())
        totals = jnp.sum(stat[...], axis=0) * (1.0 / total_width)
        mean = totals[0:1, :]
        spread_inv = lax.rsqrt(totals[1:2, :] - mean * mean + 1e-05)
        lifts = [
            (stat[owner(o), 0:1, :] * (1.0 / width) - mean) * spread_inv for o in offsets
        ]
        lifts.append(spread_inv)
        lifts.append(jnp.zeros((rows - len(lifts), rows), F32))
        columns = jnp.concatenate(lifts, axis=0).T
        inv_col = columns[:, ntp : ntp + 1]
        total = residual_ref[...].astype(F32)
        loads[7].wait()
    with jax.named_scope("act_gather"):
        waiting = [(0, 0)] + list(reversed(offsets[1:]))
        half = len(waiting) // 2
        for group in (waiting[:half], waiting[half:]):
            blocks, tall = [], []
            for o in group:
                i = number[o]
                who = owner(o)
                if i:
                    act_copies[o].wait_recv()
                value = act[i].astype(F32) * inv_col + columns[:, i : i + 1]
                value = value * stat[who, 3:4, :] + stat[who, 4:5, :]
                blocks.append(jax.nn.silu(value).astype(BF16))
                tall.append(out_weight[pl.ds(pl.multiple_of(who * width, width), width), :])
            total = total + jnp.dot(
                jnp.concatenate(blocks, axis=1),
                jnp.concatenate(tall, axis=0),
                preferred_element_type=F32,
            )
    with jax.named_scope("project"):
        meet(4)
        mixed[...] = total
        scaled_rows = (total * norm_gain_ref[...]).astype(BF16)

    with jax.named_scope("dispatch"):
        dispatch = {}
        for k in SEND_ORDER:
            outgoing[k] = jnp.dot(
                places[k * depth_rows : (k + 1) * depth_rows, :],
                scaled_rows,
                preferred_element_type=F32,
            ).astype(BF16)
            for jj in range(2 * per_side):
                d = distance(k, jj)
                part = pl.ds(jj * cap, cap)
                if d == 0:
                    xbuf[k, 0, part, :] = outgoing[k, part, :]
                else:
                    dispatch[k, jj] = send(
                        outgoing.at[k, part],
                        xbuf.at[k, 0, part],
                        z_s.at[k, jj],
                        z_r.at[k, jj],
                        (sp_at(d), t),
                    )
        pending += list(dispatch.values())
        for i in (11, 12, 13):
            loads[i].wait()

    gathers, sums, returns = {}, {}, {}

    def pass_on(k, o):
        if o == (0, 0):
            for (kk, _), copy in dispatch.items():
                if kk == k:
                    copy.wait_recv()
        else:
            gathers[k, o].wait_recv()
        for c in trees[k].children[o]:
            gathers[k, c] = send(
                xbuf.at[k, number[o]],
                xbuf.at[k, number[c]],
                ag_s.at[k, number[c]],
                ag_r.at[k, number[c]],
                (s, tp_at(c[0] - o[0], c[1] - o[1])),
            )

    def multiply(k, index):
        group, first = trees[k].groups[index], index == 0
        blocks = [xbuf[k, number[o]] for o in group]
        owners = [owner(o) for o in group]
        wide = jnp.concatenate(blocks, axis=1)
        squares = None if first else acc_sq[k]
        for block, who in zip(blocks, owners):
            plain = block.astype(F32) * stat[who, 2:3, :]
            squares = plain * plain if squares is None else squares + plain * plain
        acc_sq[k] = squares
        for weight, acc in ((expert_gate, acc_gate), (expert_up, acc_up)):
            tall = jnp.concatenate(
                [weight[pl.ds(pl.multiple_of(who * width, width), width), :] for who in owners],
                axis=0,
            )
            product = jnp.dot(wide, tall, preferred_element_type=F32)
            acc[k] = product if first else acc[k] + product

    def finish_rows(k):
        square = jnp.sum(acc_sq[k], axis=1, keepdims=True) * (1.0 / total_width)
        scale = lax.rsqrt(square + 1e-06)
        hidden = (jax.nn.silu(acc_gate[k] * scale) * (acc_up[k] * scale)).astype(BF16)
        for i in range(ntp):
            partial[k, i] = jnp.dot(
                hidden, expert_down[:, i * width : (i + 1) * width], preferred_element_type=F32
            ).astype(BF16)

    def sum_up(k, o):
        who = owner(o)
        source = partial.at[k, who]
        if trees[k].children[o]:
            value = partial[k, who].astype(F32)
            for c in trees[k].children[o]:
                sums[k, c].wait_recv()
                value = value + rs_in[k, number[c]].astype(F32)
            if o == (0, 0):
                ret_out[k] = value.astype(BF16)
                return
            rs_out[k, number[o]] = value.astype(BF16)
            source = rs_out.at[k, number[o]]
        p = trees[k].parent[o]
        sums[k, o] = send(
            source,
            rs_in.at[k, number[o]],
            rs_s.at[k, number[o]],
            rs_r.at[k, number[o]],
            (s, tp_at(p[0] - o[0], p[1] - o[1])),
        )

    def give_back(k):
        for jj in range(2 * per_side):
            d = distance(k, jj)
            part = pl.ds(jj * cap, cap)
            if d == 0:
                ret_in[k, part, :] = ret_out[k, part, :]
            else:
                returns[k, jj] = send(
                    ret_out.at[k, part],
                    ret_in.at[k, part],
                    rt_s.at[k, jj],
                    rt_r.at[k, jj],
                    (sp_at(-d), t),
                )

    along = [5.6 * (2 * k + 1) / chunks**2 for k in range(chunks)]
    arrivals, clock = {}, 0.0
    for k in SEND_ORDER:
        clock += along[k]
        arrivals[k] = clock + 1.5 + 0.75 * (8 / chunks) * (k + 1)
    for kind, k, o in plan(trees, nx, ny, depth_rows, arrivals, URGENCY):
        with jax.named_scope(f"{kind}{k}{o}"):
            if kind == "pass":
                pass_on(k, o)
            elif kind == "multiply":
                multiply(k, o)
            elif kind == "finish":
                finish_rows(k)
            else:
                sum_up(k, o)
                if o == (0, 0):
                    give_back(k)
    with jax.named_scope("wait_back"):
        for copy in returns.values():
            copy.wait_recv()
    with jax.named_scope("result"):
        answer = jnp.concatenate([ret_in[k] for k in range(chunks)], axis=0)
        result = mixed[...]
        for k in range(TOPK):
            picked = jnp.dot(picks[k], answer, preferred_element_type=F32)
            result = result + picked * route_cols[k]
        out_ref[...] = result.astype(BF16)

    pending += list(gathers.values()) + list(sums.values()) + list(returns.values())
    for copy in pending:
        copy.wait_send()


def on_device(ns, nx, ny, *args):
    (
        residual,
        glu_value,
        glu_gate,
        conv_weight,
        conv_bias,
        ln_gain,
        ln_bias,
        out_weight,
        norm_gain,
        route_ids,
        route_weight,
        expert_gate,
        expert_up,
        expert_down,
    ) = args
    ntp = nx * ny
    rows, width = residual.shape
    hidden = expert_gate.shape[2]
    capacity = 2 * rows * TOPK // ns
    slots = ns * capacity
    k, rc = CHUNKS, slots // CHUNKS
    edge = 16
    row = lambda v: v.reshape(1, -1)
    vmem = pl.BlockSpec(memory_space=pltpu.VMEM)
    hbm = pl.BlockSpec(memory_space=pltpu.HBM)
    dma = pltpu.SemaphoreType.DMA
    operands = (
        residual,
        glu_value,
        glu_gate,
        conv_weight,
        row(conv_bias),
        row(ln_gain),
        row(ln_bias),
        out_weight,
        row(norm_gain),
        route_ids.T,
        route_weight.T,
        expert_gate,
        expert_up,
        expert_down,
    )
    return pl.pallas_call(
        functools.partial(layer_kernel, ns, nx, ny),
        out_shape=jax.ShapeDtypeStruct(residual.shape, BF16),
        in_specs=[hbm] * 14,
        out_specs=vmem,
        scratch_shapes=[
            *[pltpu.VMEM(a.shape[-2:], a.dtype) for a in operands],
            pltpu.VMEM((2, edge, width), BF16),
            pltpu.VMEM((rows, width), BF16),
            pltpu.VMEM((rows + 2 * edge, width), F32),
            pltpu.VMEM((ntp, 8, width), F32),
            pltpu.VMEM((ntp, rows, width), BF16),
            pltpu.VMEM((rows, width), F32),
            pltpu.VMEM((TOPK, rows, slots), BF16),
            pltpu.VMEM((slots, rows), BF16),
            pltpu.VMEM((TOPK, rows, width), F32),
            pltpu.VMEM((k, rc, width), BF16),
            pltpu.VMEM((k, ntp, rc, width), BF16),
            pltpu.VMEM((k, rc, hidden), F32),
            pltpu.VMEM((k, rc, hidden), F32),
            pltpu.VMEM((k, rc, width), F32),
            pltpu.VMEM((k, ntp, rc, width), BF16),
            pltpu.VMEM((k, ntp, rc, width), BF16),
            pltpu.VMEM((k, ntp, rc, width), BF16),
            pltpu.VMEM((k, rc, width), BF16),
            pltpu.VMEM((k, rc, width), BF16),
            pltpu.SemaphoreType.REGULAR((4,)),
            dma((14,)),
            dma((2,)),
            dma((2,)),
            dma((ntp,)),
            dma((ntp,)),
            dma((ntp,)),
            dma((ntp,)),
            dma((k, ns // k)),
            dma((k, ns // k)),
            dma((k, ntp)),
            dma((k, ntp)),
            dma((k, ntp)),
            dma((k, ntp)),
            dma((k, ns // k)),
            dma((k, ns // k)),
        ],
        compiler_params=pltpu.CompilerParams(
            collective_id=0, has_side_effects=True, vmem_limit_bytes=66 * 1000 * 1000
        ),
        name="layer",
    )(*operands)


IN_SPECS = (
    P("sp", "tp"),
    P("sp", "tp"),
    P("sp", "tp"),
    P(None, "tp"),
    P("tp"),
    P("tp"),
    P("tp"),
    P(None, "tp"),
    P("tp"),
    P("sp", None),
    P("sp", None),
    P("sp", None, "tp"),
    P("sp", None, "tp"),
    P("sp", "tp", None),
)


def solution(mesh, nx=NX):
    ns, ntp = mesh.shape["sp"], mesh.shape["tp"]
    return jax.shard_map(
        functools.partial(on_device, ns, nx, ntp // nx),
        mesh=mesh,
        in_specs=IN_SPECS,
        out_specs=P("sp", "tp"),
        check_vma=False,
    )
```

time: 100 us -> 83.3 us (0.83)
  Pallas kernels: 92.1 us -> 81.1 us
  local copies, waits for them, and re-layouts: 7.43 us -> 1.38 us
    pallas_call x1, Pallas kernels: 92.1 us -> 81.1 us  [on_device(): pl.pallas_call(functools.partial(layer_kernel, ns, nx, ny), out_shape=jax...]
    unnamed x31 -> x1, local copies, waits for them, and re-layouts: 7.43 us -> 1.38 us
where the time goes in v2:
time: 83.3 us; the launch traced here: 82.5 us
  Pallas kernels  81.1 us (97%)
  local copies, waits for them, and re-layouts  1.38 us (2%)
    pallas_call x1, Pallas kernels, on_device(): pl.pallas_call(functools.partial(layer_kernel, ns, nx, ny), out_shape=jax...  81.1 us

profile of v2, /device:TPU:1, one launch (start us, length us, event | category | flops | bytes accessed | tf_op | source)
XLA Modules:
  0.0 82.5 jit_solution(9110962896579144286)
XLA Ops:
  0.0 81.1 %layer.1 = bf16[128,128]{1,0:T(8,128)(2,1)} custom-call(bf16[128,128]{1,0:T(8,128)(2,1)} %refs_0_.1, bf16[128,128]{1,0:T(8,128)(2,1)} %refs_1_.1, bf16[128,128]{1,0:T(8,128)(2,1)} %refs_2_.1, bf16[31,128]{1,0:T(8,128)(2,1)} %refs_3_.1, f32[1,128]{1,0:T(1,128)} %bitcast.8, f32[1,128]{1,0:T(1,128)} %bitcast.9, f32[1,128]{1,0:T(1,128)} %bitcast.10, ...), custom_call_target="tpu_custom_call" | custom-call | tf_op jit(solution)/shard_map/layer/pallas_call | solution.py:611
  81.1 1.4 %copy.16 = bf16[128,128]{1,0:T(8,128)(2,1)} copy(bf16[128,128]{1,0:T(8,128)(2,1)} %layer.1) | data formatting | bytes 65536

commit v3 on v2

--- a/solution.py
+++ b/solution.py
@@ -12,10 +12,10 @@
 F32 = jnp.float32
 BF16 = jnp.bfloat16
 NX = 4
-CHUNKS = 4
-SEND_ORDER = (0, 2, 3, 1)
-URGENCY = (1, 0, 2, 3)
-KINDS = (0, 0, 0, 1)
+CHUNKS = 8
+SEND_ORDER = (4, 5, 6, 3, 0, 7, 2, 1)
+URGENCY = (7, 3, 5, 2, 4, 0, 6, 1)
+KINDS = (0, 0, 0, 0, 1, 0, 1, 1)
 
 TREE_4X4 = {
     (1, 0): (0, 0),
@@ -84,6 +84,9 @@
             for low, high in ((0, 1), (2, 2), (3, 9))
         ]
         self.groups = [g for g in self.groups if g]
+        self.relays = [o for o in self.order if self.children[o]]
+        self.lane = {o: i for i, o in enumerate(self.relays)}
+        self.group_of = {o: i for i, g in enumerate(self.groups) for o in g}
 
 
 def signed(v, n):
@@ -145,11 +148,11 @@
                 pending.append(("multiply", k, given[k]))
                 given[k] += 1
         elif kind == "multiply":
-            now += 0.15
+            now += 0.02 + 0.001 * rows
             if given[k] == len(tree.groups) and not any(e[:2] == (kind, k) for e in pending):
                 pending.append(("finish", k, 0))
         elif kind == "finish":
-            now += 0.5
+            now += 0.1 + 0.003 * rows
             pending += [("sum", k, c) for c in tree.order if not tree.children[c]]
         else:
             now += 0.05 if tree.children[o] else 0.02
@@ -218,6 +221,7 @@
         z_r,
         ag_s,
         ag_r,
+        leaf_r,
         rs_s,
         rs_r,
         rt_s,
@@ -228,7 +232,7 @@
     total_width = ntp * width
     slots = places.shape[0]
     cap = slots // ns
-    chunks = outgoing.shape[0]
+    chunks = xbuf.shape[0]
     depth_rows = slots // chunks
     per_side = ns // (2 * chunks)
     taps = taps_ref.shape[0]
@@ -262,6 +266,9 @@
                     met.at[r], inc=1, device_id=(sp_at(d), t), device_id_type=MESH
                 )
 
+    def all_of(ref, sem):
+        return pltpu.make_async_copy(ref, ref, sem)
+
     def send(src, dst, send_sem, recv_sem, device):
         copy = pltpu.make_async_remote_copy(
             src_ref=src,
@@ -297,7 +304,58 @@
         gated[...] = gated_f.astype(BF16)
         padded[edge : edge + rows, :] = gated[...].astype(F32)
 
-        for i in (9, 3, 4, 5, 6, 8, 10, 0):
+    with jax.named_scope("barrier"):
+        pl.semaphore_wait(barrier, ntp - 1 + 2)
+        meet(0)
+
+    with jax.named_scope("halo"):
+        for side, start, d in ((0, rows - edge, 1), (1, 0, -1)):
+            send(
+                gated.at[pl.ds(start, edge)],
+                halo.at[side],
+                halo_s.at[0],
+                halo_r.at[0],
+                (sp_at(d), t),
+            )
+        meet(1)
+        all_of(halo, halo_r.at[0]).wait()
+        meet(2)
+        padded[0:edge, :] = jnp.where(s > 0, halo[0].astype(F32), 0.0)
+        padded[edge + rows : edge + rows + edge, :] = jnp.where(
+            s < ns - 1, halo[1].astype(F32), 0.0
+        )
+    with jax.named_scope("conv"):
+        for i in (3, 4, 5, 6, 8):
+            loads[i].wait()
+        tap_values = taps_ref[...].astype(F32)
+        conv = jnp.zeros((rows, width), F32) + conv_bias_ref[...]
+        for tap in range(taps):
+            start = edge - reach + tap
+            conv = conv + padded[start : start + rows, :] * tap_values[tap : tap + 1, :]
+        conv_t = conv.T
+        stat[t] = jnp.concatenate(
+            [
+                jnp.sum(conv_t, axis=0, keepdims=True),
+                jnp.sum(conv_t * conv_t, axis=0, keepdims=True),
+                1.0 / norm_gain_ref[...],
+                ln_gain_ref[...],
+                ln_bias_ref[...],
+                jnp.zeros((3, width), F32),
+            ],
+            axis=0,
+        )
+        far_first = list(reversed(offsets[1:]))
+        for o in far_first:
+            send(stat.at[t], stat.at[t], stat_s.at[0], stat_r.at[0], (s, tp_at(*o)))
+        own_mean = jnp.sum(conv, axis=1, keepdims=True) * (1.0 / width)
+        act[0] = (conv - own_mean).astype(BF16)
+        half = ntp // 2
+        for n, o in enumerate(far_first):
+            sem = act_r.at[0 if n + 1 < half else 1]
+            send(act.at[0], act.at[number[o]], act_s.at[0], sem, (s, tp_at(*o)))
+    with jax.named_scope("route"):
+        meet(3)
+        for i in (9, 10, 0):
             loads[i].wait()
         expert_of = lax.broadcasted_iota(jnp.int32, (ns, rows), 0)
         chosen = [
@@ -332,62 +390,8 @@
             both = both + here
             route_cols[k] = jnp.broadcast_to(route_weight_ref[k : k + 1, :], (width, rows)).T
         places[...] = both.astype(BF16)
-
-    with jax.named_scope("barrier"):
-        pl.semaphore_wait(barrier, ntp - 1 + 2)
-        meet(0)
-
-    with jax.named_scope("halo"):
-        to_right = send(
-            gated.at[pl.ds(rows - edge, edge)], halo.at[0], halo_s.at[0], halo_r.at[0], (sp_at(1), t)
-        )
-        to_left = send(gated.at[pl.ds(0, edge)], halo.at[1], halo_s.at[1], halo_r.at[1], (sp_at(-1), t))
-        pending = [to_right, to_left]
-        meet(1)
-        to_right.wait_recv()
-        to_left.wait_recv()
-        meet(2)
-        padded[0:edge, :] = jnp.where(s > 0, halo[0].astype(F32), 0.0)
-        padded[edge + rows : edge + rows + edge, :] = jnp.where(
-            s < ns - 1, halo[1].astype(F32), 0.0
-        )
-    with jax.named_scope("conv"):
-        tap_values = taps_ref[...].astype(F32)
-        conv = jnp.zeros((rows, width), F32) + conv_bias_ref[...]
-        for tap in range(taps):
-            start = edge - reach + tap
-            conv = conv + padded[start : start + rows, :] * tap_values[tap : tap + 1, :]
-        conv_t = conv.T
-        stat[t] = jnp.concatenate(
-            [
-                jnp.sum(conv_t, axis=0, keepdims=True),
-                jnp.sum(conv_t * conv_t, axis=0, keepdims=True),
-                1.0 / norm_gain_ref[...],
-                ln_gain_ref[...],
-                ln_bias_ref[...],
-                jnp.zeros((3, width), F32),
-            ],
-            axis=0,
-        )
-        stat_copies = []
-        for o in reversed(offsets[1:]):
-            i = number[o]
-            stat_copies.append(
-                send(stat.at[t], stat.at[t], stat_s.at[i], stat_r.at[i], (s, tp_at(*o)))
-            )
-        own_mean = jnp.sum(conv, axis=1, keepdims=True) * (1.0 / width)
-        act[0] = (conv - own_mean).astype(BF16)
-        act_copies = {}
-        for o in reversed(offsets[1:]):
-            i = number[o]
-            act_copies[o] = send(
-                act.at[0], act.at[i], act_s.at[i], act_r.at[i], (s, tp_at(*o))
-            )
     with jax.named_scope("stats"):
-        meet(3)
-        for copy in stat_copies:
-            copy.wait_recv()
-        pending += stat_copies + list(act_copies.values())
+        all_of(stat.at[pl.ds(0, ntp - 1)], stat_r.at[0]).wait()
         totals = jnp.sum(stat[...], axis=0) * (1.0 / total_width)
         mean = totals[0:1, :]
         spread_inv = lax.rsqrt(totals[1:2, :] - mean * mean + 1e-05)
@@ -401,15 +405,14 @@
         total = residual_ref[...].astype(F32)
         loads[7].wait()
     with jax.named_scope("act_gather"):
-        waiting = [(0, 0)] + list(reversed(offsets[1:]))
-        half = len(waiting) // 2
-        for group in (waiting[:half], waiting[half:]):
+        waiting = [(0, 0)] + far_first
+        for n, group in enumerate((waiting[:half], waiting[half:])):
             blocks, tall = [], []
+            if n == 1 or half > 1:
+                all_of(act.at[pl.ds(0, half - 1 + n)], act_r.at[n]).wait()
             for o in group:
                 i = number[o]
                 who = owner(o)
-                if i:
-                    act_copies[o].wait_recv()
                 value = act[i].astype(F32) * inv_col + columns[:, i : i + 1]
                 value = value * stat[who, 3:4, :] + stat[who, 4:5, :]
                 blocks.append(jax.nn.silu(value).astype(BF16))
@@ -425,50 +428,55 @@
         scaled_rows = (total * norm_gain_ref[...]).astype(BF16)
 
     with jax.named_scope("dispatch"):
-        dispatch = {}
         for k in SEND_ORDER:
-            outgoing[k] = jnp.dot(
-                places[k * depth_rows : (k + 1) * depth_rows, :],
-                scaled_rows,
-                preferred_element_type=F32,
+            chunk = pl.ds(k * depth_rows, depth_rows)
+            outgoing[chunk, :] = jnp.dot(
+                places[chunk, :], scaled_rows, preferred_element_type=F32
             ).astype(BF16)
             for jj in range(2 * per_side):
                 d = distance(k, jj)
-                part = pl.ds(jj * cap, cap)
+                part, flat = pl.ds(jj * cap, cap), pl.ds(k * depth_rows + jj * cap, cap)
                 if d == 0:
-                    xbuf[k, 0, part, :] = outgoing[k, part, :]
+                    xbuf[k, 0, part, :] = outgoing[flat, :]
                 else:
-                    dispatch[k, jj] = send(
-                        outgoing.at[k, part],
-                        xbuf.at[k, 0, part],
-                        z_s.at[k, jj],
-                        z_r.at[k, jj],
-                        (sp_at(d), t),
+                    send(
+                        outgoing.at[flat], xbuf.at[k, 0, part], z_s.at[0], z_r.at[k], (sp_at(d), t)
                     )
-        pending += list(dispatch.values())
         for i in (11, 12, 13):
             loads[i].wait()
 
-    gathers, sums, returns = {}, {}, {}
+    def blocks_of(buffer, k, count):
+        return buffer.at[k, pl.ds(0, count)]
+
+    def arriving_leaves(k, index):
+        tree = trees[k]
+        return [o for o in tree.groups[index] if o != (0, 0) and not tree.children[o]]
 
     def pass_on(k, o):
+        tree = trees[k]
         if o == (0, 0):
-            for (kk, _), copy in dispatch.items():
-                if kk == k:
-                    copy.wait_recv()
-        else:
-            gathers[k, o].wait_recv()
-        for c in trees[k].children[o]:
-            gathers[k, c] = send(
+            here = cap if distance(k, 0) == 0 else 0
+            all_of(xbuf.at[k, 0, pl.ds(0, depth_rows - here)], z_r.at[k]).wait()
+        elif tree.children[o]:
+            all_of(xbuf.at[k, number[o]], ag_r.at[k, tree.lane[o] - 1]).wait()
+        for c in tree.children[o]:
+            if tree.children[c]:
+                sem = ag_r.at[k, tree.lane[c] - 1]
+            else:
+                sem = leaf_r.at[k, tree.group_of[c]]
+            send(
                 xbuf.at[k, number[o]],
                 xbuf.at[k, number[c]],
-                ag_s.at[k, number[c]],
-                ag_r.at[k, number[c]],
+                ag_s.at[0],
+                sem,
                 (s, tp_at(c[0] - o[0], c[1] - o[1])),
             )
 
     def multiply(k, index):
         group, first = trees[k].groups[index], index == 0
+        leaves = arriving_leaves(k, index)
+        if leaves:
+            all_of(blocks_of(xbuf, k, len(leaves)), leaf_r.at[k, index]).wait()
         blocks = [xbuf[k, number[o]] for o in group]
         owners = [owner(o) for o in group]
         wide = jnp.concatenate(blocks, axis=1)
@@ -496,40 +504,36 @@
 
     def sum_up(k, o):
         who = owner(o)
+        tree = trees[k]
         source = partial.at[k, who]
-        if trees[k].children[o]:
+        if tree.children[o]:
+            count = len(tree.children[o])
+            all_of(blocks_of(rs_in, k, count), rs_r.at[k, tree.lane[o]]).wait()
             value = partial[k, who].astype(F32)
-            for c in trees[k].children[o]:
-                sums[k, c].wait_recv()
+            for c in tree.children[o]:
                 value = value + rs_in[k, number[c]].astype(F32)
             if o == (0, 0):
-                ret_out[k] = value.astype(BF16)
+                ret_out[pl.ds(k * depth_rows, depth_rows), :] = value.astype(BF16)
                 return
             rs_out[k, number[o]] = value.astype(BF16)
             source = rs_out.at[k, number[o]]
-        p = trees[k].parent[o]
-        sums[k, o] = send(
+        p = tree.parent[o]
+        send(
             source,
             rs_in.at[k, number[o]],
-            rs_s.at[k, number[o]],
-            rs_r.at[k, number[o]],
+            rs_s.at[0],
+            rs_r.at[k, tree.lane[p]],
             (s, tp_at(p[0] - o[0], p[1] - o[1])),
         )
 
     def give_back(k):
         for jj in range(2 * per_side):
             d = distance(k, jj)
-            part = pl.ds(jj * cap, cap)
+            part = pl.ds(k * depth_rows + jj * cap, cap)
             if d == 0:
-                ret_in[k, part, :] = ret_out[k, part, :]
+                ret_in[part, :] = ret_out[part, :]
             else:
-                returns[k, jj] = send(
-                    ret_out.at[k, part],
-                    ret_in.at[k, part],
-                    rt_s.at[k, jj],
-                    rt_r.at[k, jj],
-                    (sp_at(-d), t),
-                )
+                send(ret_out.at[part], ret_in.at[part], rt_s.at[0], rt_r.at[0], (sp_at(-d), t))
 
     along = [5.6 * (2 * k + 1) / chunks**2 for k in range(chunks)]
     arrivals, clock = {}, 0.0
@@ -548,20 +552,26 @@
                 sum_up(k, o)
                 if o == (0, 0):
                     give_back(k)
+    away_rows = pl.ds(0, slots - cap)
+    with jax.named_scope("wait_sends"):
+        all_of(halo, halo_s.at[0]).wait()
+        all_of(stat.at[pl.ds(0, ntp - 1)], stat_s.at[0]).wait()
+        all_of(act.at[pl.ds(0, ntp - 1)], act_s.at[0]).wait()
+        all_of(outgoing.at[away_rows], z_s.at[0]).wait()
+        all_of(xbuf.at[:, pl.ds(0, ntp - 1)], ag_s.at[0]).wait()
+        all_of(rs_in.at[:, pl.ds(0, ntp - 1)], rs_s.at[0]).wait()
     with jax.named_scope("wait_back"):
-        for copy in returns.values():
-            copy.wait_recv()
+        all_of(ret_in.at[away_rows], rt_r.at[0]).wait()
     with jax.named_scope("result"):
-        answer = jnp.concatenate([ret_in[k] for k in range(chunks)], axis=0)
+        answer = ret_in[...]
         result = mixed[...]
         for k in range(TOPK):
             picked = jnp.dot(picks[k], answer, preferred_element_type=F32)
             result = result + picked * route_cols[k]
         out_ref[...] = result.astype(BF16)
 
-    pending += list(gathers.values()) + list(sums.values()) + list(returns.values())
-    for copy in pending:
-        copy.wait_send()
+    with jax.named_scope("end"):
+        all_of(ret_out.at[away_rows], rt_s.at[0]).wait()
 
 
 def on_device(ns, nx, ny, *args):
@@ -624,7 +634,7 @@
             pltpu.VMEM((TOPK, rows, slots), BF16),
             pltpu.VMEM((slots, rows), BF16),
             pltpu.VMEM((TOPK, rows, width), F32),
-            pltpu.VMEM((k, rc, width), BF16),
+            pltpu.VMEM((slots, width), BF16),
             pltpu.VMEM((k, ntp, rc, width), BF16),
             pltpu.VMEM((k, rc, hidden), F32),
             pltpu.VMEM((k, rc, hidden), F32),
@@ -632,24 +642,25 @@
             pltpu.VMEM((k, ntp, rc, width), BF16),
             pltpu.VMEM((k, ntp, rc, width), BF16),
             pltpu.VMEM((k, ntp, rc, width), BF16),
-            pltpu.VMEM((k, rc, width), BF16),
-            pltpu.VMEM((k, rc, width), BF16),
+            pltpu.VMEM((slots, width), BF16),
+            pltpu.VMEM((slots, width), BF16),
             pltpu.SemaphoreType.REGULAR((4,)),
             dma((14,)),
+            dma((1,)),
+            dma((1,)),
+            dma((1,)),
+            dma((1,)),
+            dma((1,)),
             dma((2,)),
-            dma((2,)),
-            dma((ntp,)),
-            dma((ntp,)),
-            dma((ntp,)),
-            dma((ntp,)),
-            dma((k, ns // k)),
-            dma((k, ns // k)),
-            dma((k, ntp)),
-            dma((k, ntp)),
-            dma((k, ntp)),
-            dma((k, ntp)),
-            dma((k, ns // k)),
-            dma((k, ns // k)),
+            dma((1,)),
+            dma((k,)),
+            dma((1,)),
+            dma((k, 9)),
+            dma((k, 3)),
+            dma((1,)),
+            dma((k, 10)),
+            dma((1,)),
+            dma((1,)),
         ],
         compiler_params=pltpu.CompilerParams(
             collective_id=0, has_side_effects=True, vmem_limit_bytes=66 * 1000 * 1000

time: 83.3 us -> 76.6 us (0.920)
  Pallas kernels: 81.1 us -> 75 us
    pallas_call x1, Pallas kernels: 81.1 us -> 75 us  [on_device(): pl.pallas_call(functools.partial(layer_kernel, ns, nx, ny), out_shape=jax...]
where the time goes in v3:
time: 76.6 us; the launch traced here: 76.4 us
  Pallas kernels  75 us (98%)
  local copies, waits for them, and re-layouts  1.38 us (2%)
    pallas_call x1, Pallas kernels, on_device(): pl.pallas_call(functools.partial(layer_kernel, ns, nx, ny), out_shape=jax...  75 us

profile of v3, /device:TPU:1, one launch (start us, length us, event | category | flops | bytes accessed | tf_op | source)
XLA Modules:
  0.0 76.4 jit_solution(6943484155893170391)
XLA Ops:
  0.0 75.0 %layer.1 = bf16[128,128]{1,0:T(8,128)(2,1)} custom-call(bf16[128,128]{1,0:T(8,128)(2,1)} %refs_0_.1, bf16[128,128]{1,0:T(8,128)(2,1)} %refs_1_.1, bf16[128,128]{1,0:T(8,128)(2,1)} %refs_2_.1, bf16[31,128]{1,0:T(8,128)(2,1)} %refs_3_.1, f32[1,128]{1,0:T(1,128)} %bitcast.8, f32[1,128]{1,0:T(1,128)} %bitcast.9, f32[1,128]{1,0:T(1,128)} %bitcast.10, ...), custom_call_target="tpu_custom_call" | custom-call | tf_op jit(solution)/shard_map/layer/pallas_call | solution.py:621
  75.1 1.4 %copy.16 = bf16[128,128]{1,0:T(8,128)(2,1)} copy(bf16[128,128]{1,0:T(8,128)(2,1)} %layer.1) | data formatting | bytes 65536

commit v4 on v3

--- a/solution.py
+++ b/solution.py
@@ -13,9 +13,11 @@
 BF16 = jnp.bfloat16
 NX = 4
 CHUNKS = 8
-SEND_ORDER = (4, 5, 6, 3, 0, 7, 2, 1)
-URGENCY = (7, 3, 5, 2, 4, 0, 6, 1)
-KINDS = (0, 0, 0, 0, 1, 0, 1, 1)
+SEND_ORDER = (1, 2, 3, 4, 0, 7, 6, 5)
+URGENCY = (6, 2, 7, 5, 0, 4, 1, 3)
+SUM_URGENCY = (6, 5, 7, 1, 3, 4, 2, 0)
+KINDS = (0, 0, 1, 1, 0, 1, 1, 1)
+LEAD = 0.3
 
 TREE_4X4 = {
     (1, 0): (0, 0),
@@ -44,6 +46,7 @@
     (3, 2): (3, 1),
     (2, 2): (1, 1),
 }
+DIRECT_4X4 = {o: (0, 0) for o in TREE_4X4}
 
 
 def turned(tree, quarters):
@@ -58,7 +61,7 @@
 class Tree:
     def __init__(self, nx, ny, kind, quarters):
         if (nx, ny) == (4, 4):
-            parent = turned(SHALLOW_4X4 if kind else TREE_4X4, quarters)
+            parent = turned((TREE_4X4, SHALLOW_4X4, DIRECT_4X4)[kind], quarters)
         else:
             parent, frontier = {}, [(0, 0)]
             while frontier:
@@ -93,7 +96,7 @@
     return (v + n // 2 - 1) % n - (n // 2 - 1)
 
 
-def plan(trees, nx, ny, rows, arrivals, urgency):
+def plan(trees, nx, ny, rows, arrivals, urgency, sum_urgency, lead):
     wire, latency, hop = rows * 256 / 46.65e3, 2.2, 0.75
     link, now, steps, pending = {}, 0.0, [], []
     arrived, summed, passed, given = {}, {}, {}, {}
@@ -107,6 +110,10 @@
                     link[axis, way] = max(link.get((axis, way), 0.0), now) + wire
                     end = max(end, link[axis, way])
         return end + latency + hop * (abs(dx) + abs(dy) - 1)
+
+    def way(p, o):
+        dx, dy = signed(o[0] - p[0], nx), signed(o[1] - p[1], ny)
+        return (0, 1 if dx > 0 else -1) if dx else (1, 1 if dy > 0 else -1)
 
     for k in range(len(trees)):
         pending.append(("pass", k, (0, 0)))
@@ -118,15 +125,21 @@
             kind, k, o = e
             if kind == "pass":
                 ready[e] = arrived[k, o] if o != (0, 0) else arrivals[k]
+                ways = [way(o, c) for c in trees[k].children[o]]
             elif kind == "sum":
                 ready[e] = max([summed[k, c] for c in trees[k].children[o]], default=0.0)
+                ways = [way(o, trees[k].parent[o])] if o != (0, 0) else []
             else:
                 ready[e] = 0.0
+                ways = []
+            if ways:
+                ready[e] = max(ready[e], min(link.get(w, 0.0) for w in ways) - lead)
 
         def rank(e):
             kind, k, o = e
             late = -trees[k].depth[o] if kind == "sum" else 0
-            return ({"pass": 0, "sum": 0, "finish": 1}.get(kind, 2), urgency[k], late, str(o))
+            first = (sum_urgency if kind == "sum" else urgency)[k]
+            return ({"pass": 0, "sum": 0, "finish": 1}.get(kind, 2), first, late, str(o))
 
         able = [e for e in pending if ready[e] <= now + 1e-9]
         if able:
@@ -194,6 +207,7 @@
         gated,
         padded,
         stat,
+        gains,
         act,
         mixed,
         picks,
@@ -317,15 +331,29 @@
                 halo_r.at[0],
                 (sp_at(d), t),
             )
+        far_first = list(reversed(offsets[1:]))
+        for i in (5, 6, 8):
+            loads[i].wait()
+        gains[t] = jnp.concatenate(
+            [
+                jnp.zeros((2, width), F32),
+                1.0 / norm_gain_ref[...],
+                ln_gain_ref[...],
+                ln_bias_ref[...],
+                jnp.zeros((3, width), F32),
+            ],
+            axis=0,
+        )
+        for o in far_first:
+            send(gains.at[t], gains.at[t], stat_s.at[0], stat_r.at[0], (s, tp_at(*o)))
         meet(1)
         all_of(halo, halo_r.at[0]).wait()
-        meet(2)
         padded[0:edge, :] = jnp.where(s > 0, halo[0].astype(F32), 0.0)
         padded[edge + rows : edge + rows + edge, :] = jnp.where(
             s < ns - 1, halo[1].astype(F32), 0.0
         )
     with jax.named_scope("conv"):
-        for i in (3, 4, 5, 6, 8):
+        for i in (3, 4):
             loads[i].wait()
         tap_values = taps_ref[...].astype(F32)
         conv = jnp.zeros((rows, width), F32) + conv_bias_ref[...]
@@ -333,20 +361,11 @@
             start = edge - reach + tap
             conv = conv + padded[start : start + rows, :] * tap_values[tap : tap + 1, :]
         conv_t = conv.T
-        stat[t] = jnp.concatenate(
-            [
-                jnp.sum(conv_t, axis=0, keepdims=True),
-                jnp.sum(conv_t * conv_t, axis=0, keepdims=True),
-                1.0 / norm_gain_ref[...],
-                ln_gain_ref[...],
-                ln_bias_ref[...],
-                jnp.zeros((3, width), F32),
-            ],
-            axis=0,
-        )
-        far_first = list(reversed(offsets[1:]))
+        stat[t, 0:1, :] = jnp.sum(conv_t, axis=0, keepdims=True)
+        stat[t, 1:2, :] = jnp.sum(conv_t * conv_t, axis=0, keepdims=True)
+        sums_here = stat.at[t, pl.ds(0, 2)]
         for o in far_first:
-            send(stat.at[t], stat.at[t], stat_s.at[0], stat_r.at[0], (s, tp_at(*o)))
+            send(sums_here, sums_here, stat_s.at[1], stat_r.at[1], (s, tp_at(*o)))
         own_mean = jnp.sum(conv, axis=1, keepdims=True) * (1.0 / width)
         act[0] = (conv - own_mean).astype(BF16)
         half = ntp // 2
@@ -354,7 +373,7 @@
             sem = act_r.at[0 if n + 1 < half else 1]
             send(act.at[0], act.at[number[o]], act_s.at[0], sem, (s, tp_at(*o)))
     with jax.named_scope("route"):
-        meet(3)
+        meet(2)
         for i in (9, 10, 0):
             loads[i].wait()
         expert_of = lax.broadcasted_iota(jnp.int32, (ns, rows), 0)
@@ -391,8 +410,10 @@
             route_cols[k] = jnp.broadcast_to(route_weight_ref[k : k + 1, :], (width, rows)).T
         places[...] = both.astype(BF16)
     with jax.named_scope("stats"):
-        all_of(stat.at[pl.ds(0, ntp - 1)], stat_r.at[0]).wait()
-        totals = jnp.sum(stat[...], axis=0) * (1.0 / total_width)
+        meet(3)
+        all_of(gains.at[pl.ds(0, ntp - 1)], stat_r.at[0]).wait()
+        all_of(stat.at[pl.ds(0, ntp - 1), pl.ds(0, 2)], stat_r.at[1]).wait()
+        totals = jnp.sum(stat[:, 0:2, :], axis=0) * (1.0 / total_width)
         mean = totals[0:1, :]
         spread_inv = lax.rsqrt(totals[1:2, :] - mean * mean + 1e-05)
         lifts = [
@@ -414,7 +435,7 @@
                 i = number[o]
                 who = owner(o)
                 value = act[i].astype(F32) * inv_col + columns[:, i : i + 1]
-                value = value * stat[who, 3:4, :] + stat[who, 4:5, :]
+                value = value * gains[who, 3:4, :] + gains[who, 4:5, :]
                 blocks.append(jax.nn.silu(value).astype(BF16))
                 tall.append(out_weight[pl.ds(pl.multiple_of(who * width, width), width), :])
             total = total + jnp.dot(
@@ -428,11 +449,8 @@
         scaled_rows = (total * norm_gain_ref[...]).astype(BF16)
 
     with jax.named_scope("dispatch"):
+        outgoing[...] = jnp.dot(places[...], scaled_rows, preferred_element_type=F32).astype(BF16)
         for k in SEND_ORDER:
-            chunk = pl.ds(k * depth_rows, depth_rows)
-            outgoing[chunk, :] = jnp.dot(
-                places[chunk, :], scaled_rows, preferred_element_type=F32
-            ).astype(BF16)
             for jj in range(2 * per_side):
                 d = distance(k, jj)
                 part, flat = pl.ds(jj * cap, cap), pl.ds(k * depth_rows + jj * cap, cap)
@@ -482,7 +500,7 @@
         wide = jnp.concatenate(blocks, axis=1)
         squares = None if first else acc_sq[k]
         for block, who in zip(blocks, owners):
-            plain = block.astype(F32) * stat[who, 2:3, :]
+            plain = block.astype(F32) * gains[who, 2:3, :]
             squares = plain * plain if squares is None else squares + plain * plain
         acc_sq[k] = squares
         for weight, acc in ((expert_gate, acc_gate), (expert_up, acc_up)):
@@ -497,10 +515,12 @@
         square = jnp.sum(acc_sq[k], axis=1, keepdims=True) * (1.0 / total_width)
         scale = lax.rsqrt(square + 1e-06)
         hidden = (jax.nn.silu(acc_gate[k] * scale) * (acc_up[k] * scale)).astype(BF16)
-        for i in range(ntp):
-            partial[k, i] = jnp.dot(
-                hidden, expert_down[:, i * width : (i + 1) * width], preferred_element_type=F32
+        for i in range(0, ntp, 2):
+            pair = jnp.dot(
+                hidden, expert_down[:, i * width : (i + 2) * width], preferred_element_type=F32
             ).astype(BF16)
+            partial[k, i] = pair[:, :width]
+            partial[k, i + 1] = pair[:, width:]
 
     def sum_up(k, o):
         who = owner(o)
@@ -539,8 +559,8 @@
     arrivals, clock = {}, 0.0
     for k in SEND_ORDER:
         clock += along[k]
-        arrivals[k] = clock + 1.5 + 0.75 * (8 / chunks) * (k + 1)
-    for kind, k, o in plan(trees, nx, ny, depth_rows, arrivals, URGENCY):
+        arrivals[k] = clock + 1.7 + 0.8 * (8 / chunks) * (k + 1)
+    for kind, k, o in plan(trees, nx, ny, depth_rows, arrivals, URGENCY, SUM_URGENCY, LEAD):
         with jax.named_scope(f"{kind}{k}{o}"):
             if kind == "pass":
                 pass_on(k, o)
@@ -555,7 +575,8 @@
     away_rows = pl.ds(0, slots - cap)
     with jax.named_scope("wait_sends"):
         all_of(halo, halo_s.at[0]).wait()
-        all_of(stat.at[pl.ds(0, ntp - 1)], stat_s.at[0]).wait()
+        all_of(gains.at[pl.ds(0, ntp - 1)], stat_s.at[0]).wait()
+        all_of(stat.at[pl.ds(0, ntp - 1), pl.ds(0, 2)], stat_s.at[1]).wait()
         all_of(act.at[pl.ds(0, ntp - 1)], act_s.at[0]).wait()
         all_of(outgoing.at[away_rows], z_s.at[0]).wait()
         all_of(xbuf.at[:, pl.ds(0, ntp - 1)], ag_s.at[0]).wait()
@@ -629,6 +650,7 @@
             pltpu.VMEM((rows, width), BF16),
             pltpu.VMEM((rows + 2 * edge, width), F32),
             pltpu.VMEM((ntp, 8, width), F32),
+            pltpu.VMEM((ntp, 8, width), F32),
             pltpu.VMEM((ntp, rows, width), BF16),
             pltpu.VMEM((rows, width), F32),
             pltpu.VMEM((TOPK, rows, slots), BF16),
@@ -648,8 +670,8 @@
             dma((14,)),
             dma((1,)),
             dma((1,)),
-            dma((1,)),
-            dma((1,)),
+            dma((2,)),
+            dma((2,)),
             dma((1,)),
             dma((2,)),
             dma((1,)),

time: 76.6 us -> 74.2 us (0.969)
  Pallas kernels: 75 us -> 72.7 us
    pallas_call x1, Pallas kernels: 75 us -> 72.7 us  [on_device(): pl.pallas_call(functools.partial(layer_kernel, ns, nx, ny), out_shape=jax...]
where the time goes in v4:
time: 74.2 us; the launch traced here: 74 us
  Pallas kernels  72.7 us (98%)
  local copies, waits for them, and re-layouts  1.38 us (2%)
    pallas_call x1, Pallas kernels, on_device(): pl.pallas_call(functools.partial(layer_kernel, ns, nx, ny), out_shape=jax...  72.7 us

profile of v4, /device:TPU:1, one launch (start us, length us, event | category | flops | bytes accessed | tf_op | source)
XLA Modules:
  0.0 74.0 jit_solution(4803501353137446967)
XLA Ops:
  0.0 72.7 %layer.1 = bf16[128,128]{1,0:T(8,128)(2,1)} custom-call(bf16[128,128]{1,0:T(8,128)(2,1)} %refs_0_.1, bf16[128,128]{1,0:T(8,128)(2,1)} %refs_1_.1, bf16[128,128]{1,0:T(8,128)(2,1)} %refs_2_.1, bf16[31,128]{1,0:T(8,128)(2,1)} %refs_3_.1, f32[1,128]{1,0:T(1,128)} %bitcast.8, f32[1,128]{1,0:T(1,128)} %bitcast.9, f32[1,128]{1,0:T(1,128)} %bitcast.10, ...), custom_call_target="tpu_custom_call" | custom-call | tf_op jit(solution)/shard_map/layer/pallas_call | solution.py:642
  72.7 1.4 %copy.16 = bf16[128,128]{1,0:T(8,128)(2,1)} copy(bf16[128,128]{1,0:T(8,128)(2,1)} %layer.1) | data formatting | bytes 65536

commit v5 on v4

--- a/solution.py
+++ b/solution.py
@@ -13,11 +13,11 @@
 BF16 = jnp.bfloat16
 NX = 4
 CHUNKS = 8
-SEND_ORDER = (1, 2, 3, 4, 0, 7, 6, 5)
-URGENCY = (6, 2, 7, 5, 0, 4, 1, 3)
-SUM_URGENCY = (6, 5, 7, 1, 3, 4, 2, 0)
-KINDS = (0, 0, 1, 1, 0, 1, 1, 1)
-LEAD = 0.3
+SEND_ORDER = (0, 2, 7, 3, 1, 6, 4, 5)
+URGENCY = (2, 6, 7, 5, 4, 3, 1, 0)
+SUM_URGENCY = (4, 5, 3, 6, 7, 1, 0, 2)
+KINDS = (1, 1, 1, 1, 1, 1, 1, 1)
+LEAD = 0.7
 
 TREE_4X4 = {
     (1, 0): (0, 0),
@@ -87,9 +87,22 @@
             for low, high in ((0, 1), (2, 2), (3, 9))
         ]
         self.groups = [g for g in self.groups if g]
-        self.relays = [o for o in self.order if self.children[o]]
-        self.lane = {o: i for i, o in enumerate(self.relays)}
-        self.group_of = {o: i for i, g in enumerate(self.groups) for o in g}
+        relays = [o for o in self.order if self.children[o]]
+        leaf_groups = [
+            i for i, g in enumerate(self.groups) if any(not self.children[o] for o in g)
+        ]
+        group_of = {o: i for i, g in enumerate(self.groups) for o in g}
+        self.lane = {o: i - 1 for i, o in enumerate(relays)}
+        for o in self.order:
+            if o not in self.lane:
+                self.lane[o] = len(relays) - 1 + leaf_groups.index(group_of[o])
+        self.lanes = len(relays) - 1 + len(leaf_groups)
+        self.sum_lane = {o: i for i, o in enumerate(relays)}
+        self.sum_lanes = len(relays)
+
+
+def chunk_trees(nx, ny):
+    return [Tree(nx, ny, KINDS[k], k) for k in range(CHUNKS)]
 
 
 def signed(v, n):
@@ -97,7 +110,7 @@
 
 
 def plan(trees, nx, ny, rows, arrivals, urgency, sum_urgency, lead):
-    wire, latency, hop = rows * 256 / 46.65e3, 2.2, 0.75
+    wire, latency, hop = rows * 256 / 46.65e3, 2.6, 0.75
     link, now, steps, pending = {}, 0.0, [], []
     arrived, summed, passed, given = {}, {}, {}, {}
 
@@ -155,17 +168,17 @@
             for c in tree.children[o]:
                 arrived[k, c] = sent(o, c)
                 pending.append(("pass", k, c))
-            now += 0.03
+            now += 0.04
             passed[k].add(o)
             while given[k] < len(tree.groups) and passed[k].issuperset(tree.groups[given[k]]):
                 pending.append(("multiply", k, given[k]))
                 given[k] += 1
         elif kind == "multiply":
-            now += 0.02 + 0.001 * rows
+            now += 0.15
             if given[k] == len(tree.groups) and not any(e[:2] == (kind, k) for e in pending):
                 pending.append(("finish", k, 0))
         elif kind == "finish":
-            now += 0.1 + 0.003 * rows
+            now += 0.38
             pending += [("sum", k, c) for c in tree.order if not tree.children[c]]
         else:
             now += 0.05 if tree.children[o] else 0.02
@@ -235,7 +248,6 @@
         z_r,
         ag_s,
         ag_r,
-        leaf_r,
         rs_s,
         rs_r,
         rt_s,
@@ -255,7 +267,9 @@
     s = lax.axis_index("sp")
     t = lax.axis_index("tp")
     ty, tx = t // nx, lax.rem(t, nx)
-    trees = [Tree(nx, ny, KINDS[k], k) for k in range(chunks)]
+    trees = chunk_trees(nx, ny)
+    ag_base = [sum(tree.lanes for tree in trees[:k]) for k in range(chunks)]
+    rs_base = [sum(tree.sum_lanes for tree in trees[:k]) for k in range(chunks)]
     offsets = sorted(trees[0].order, key=lambda o: (abs(signed(o[0], nx)) + abs(signed(o[1], ny)), o))
     number = {o: i for i, o in enumerate(offsets)}
 
@@ -476,12 +490,9 @@
             here = cap if distance(k, 0) == 0 else 0
             all_of(xbuf.at[k, 0, pl.ds(0, depth_rows - here)], z_r.at[k]).wait()
         elif tree.children[o]:
-            all_of(xbuf.at[k, number[o]], ag_r.at[k, tree.lane[o] - 1]).wait()
+            all_of(xbuf.at[k, number[o]], ag_r.at[ag_base[k] + tree.lane[o]]).wait()
         for c in tree.children[o]:
-            if tree.children[c]:
-                sem = ag_r.at[k, tree.lane[c] - 1]
-            else:
-                sem = leaf_r.at[k, tree.group_of[c]]
+            sem = ag_r.at[ag_base[k] + tree.lane[c]]
             send(
                 xbuf.at[k, number[o]],
                 xbuf.at[k, number[c]],
@@ -494,7 +505,8 @@
         group, first = trees[k].groups[index], index == 0
         leaves = arriving_leaves(k, index)
         if leaves:
-            all_of(blocks_of(xbuf, k, len(leaves)), leaf_r.at[k, index]).wait()
+            sem = ag_r.at[ag_base[k] + trees[k].lane[leaves[0]]]
+            all_of(blocks_of(xbuf, k, len(leaves)), sem).wait()
         blocks = [xbuf[k, number[o]] for o in group]
         owners = [owner(o) for o in group]
         wide = jnp.concatenate(blocks, axis=1)
@@ -528,7 +540,7 @@
         source = partial.at[k, who]
         if tree.children[o]:
             count = len(tree.children[o])
-            all_of(blocks_of(rs_in, k, count), rs_r.at[k, tree.lane[o]]).wait()
+            all_of(blocks_of(rs_in, k, count), rs_r.at[rs_base[k] + tree.sum_lane[o]]).wait()
             value = partial[k, who].astype(F32)
             for c in tree.children[o]:
                 value = value + rs_in[k, number[c]].astype(F32)
@@ -542,7 +554,7 @@
             source,
             rs_in.at[k, number[o]],
             rs_s.at[0],
-            rs_r.at[k, tree.lane[p]],
+            rs_r.at[rs_base[k] + tree.sum_lane[p]],
             (s, tp_at(p[0] - o[0], p[1] - o[1])),
         )
 
@@ -677,10 +689,9 @@
             dma((1,)),
             dma((k,)),
             dma((1,)),
-            dma((k, 9)),
-            dma((k, 3)),
+            dma((sum(tree.lanes for tree in chunk_trees(nx, ny)),)),
             dma((1,)),
-            dma((k, 10)),
+            dma((sum(tree.sum_lanes for tree in chunk_trees(nx, ny)),)),
             dma((1,)),
             dma((1,)),
         ],

time: 74.2 us -> 71.7 us (0.966)
  Pallas kernels: 72.7 us -> 70.1 us
    pallas_call x1, Pallas kernels: 72.7 us -> 70.1 us  [on_device(): pl.pallas_call(functools.partial(layer_kernel, ns, nx, ny), out_shape=jax...]
where the time goes in v5:
time: 71.7 us; the launch traced here: 71.5 us
  Pallas kernels  70.1 us (98%)
  local copies, waits for them, and re-layouts  1.38 us (2%)
    pallas_call x1, Pallas kernels, on_device(): pl.pallas_call(functools.partial(layer_kernel, ns, nx, ny), out_shape=jax...  70.1 us

profile of v5, /device:TPU:1, one launch (start us, length us, event | category | flops | bytes accessed | tf_op | source)
XLA Modules:
  0.0 71.5 jit_solution(8116543842649043178)
XLA Ops:
  0.0 70.1 %layer.1 = bf16[128,128]{1,0:T(8,128)(2,1)} custom-call(bf16[128,128]{1,0:T(8,128)(2,1)} %refs_0_.1, bf16[128,128]{1,0:T(8,128)(2,1)} %refs_1_.1, bf16[128,128]{1,0:T(8,128)(2,1)} %refs_2_.1, bf16[31,128]{1,0:T(8,128)(2,1)} %refs_3_.1, f32[1,128]{1,0:T(1,128)} %bitcast.8, f32[1,128]{1,0:T(1,128)} %bitcast.9, f32[1,128]{1,0:T(1,128)} %bitcast.10, ...), custom_call_target="tpu_custom_call" | custom-call | tf_op jit(solution)/shard_map/layer/pallas_call | solution.py:654
  70.1 1.4 %copy.16 = bf16[128,128]{1,0:T(8,128)(2,1)} copy(bf16[128,128]{1,0:T(8,128)(2,1)} %layer.1) | data formatting | bytes 65536

commit v6 on v5

--- a/solution.py
+++ b/solution.py
@@ -13,11 +13,11 @@
 BF16 = jnp.bfloat16
 NX = 4
 CHUNKS = 8
-SEND_ORDER = (0, 2, 7, 3, 1, 6, 4, 5)
-URGENCY = (2, 6, 7, 5, 4, 3, 1, 0)
-SUM_URGENCY = (4, 5, 3, 6, 7, 1, 0, 2)
+SEND_ORDER = (1, 7, 4, 0, 2, 3, 6, 5)
+URGENCY = (6, 0, 3, 7, 4, 2, 1, 5)
+SUM_URGENCY = (5, 7, 6, 1, 4, 3, 2, 0)
 KINDS = (1, 1, 1, 1, 1, 1, 1, 1)
-LEAD = 0.7
+LEAD = 0.3
 
 TREE_4X4 = {
     (1, 0): (0, 0),
@@ -110,7 +110,7 @@
 
 
 def plan(trees, nx, ny, rows, arrivals, urgency, sum_urgency, lead):
-    wire, latency, hop = rows * 256 / 46.65e3, 2.6, 0.75
+    wire, latency, hop = rows * 256 / 46.65e3, 3.2, 0.75
     link, now, steps, pending = {}, 0.0, [], []
     arrived, summed, passed, given = {}, {}, {}, {}
 

time: 71.7 us -> 71.4 us (level)
  no operation moved by 1% of the time
where the time goes in v6:
time: 71.4 us; the launch traced here: 71.3 us
  Pallas kernels  69.9 us (98%)
  local copies, waits for them, and re-layouts  1.38 us (2%)
    pallas_call x1, Pallas kernels, on_device(): pl.pallas_call(functools.partial(layer_kernel, ns, nx, ny), out_shape=jax...  69.9 us

profile of v6, /device:TPU:1, one launch (start us, length us, event | category | flops | bytes accessed | tf_op | source)
XLA Modules:
  0.0 71.3 jit_solution(169931337236434307)
XLA Ops:
  0.0 69.9 %layer.1 = bf16[128,128]{1,0:T(8,128)(2,1)} custom-call(bf16[128,128]{1,0:T(8,128)(2,1)} %refs_0_.1, bf16[128,128]{1,0:T(8,128)(2,1)} %refs_1_.1, bf16[128,128]{1,0:T(8,128)(2,1)} %refs_2_.1, bf16[31,128]{1,0:T(8,128)(2,1)} %refs_3_.1, f32[1,128]{1,0:T(1,128)} %bitcast.8, f32[1,128]{1,0:T(1,128)} %bitcast.9, f32[1,128]{1,0:T(1,128)} %bitcast.10, ...), custom_call_target="tpu_custom_call" | custom-call | tf_op jit(solution)/shard_map/layer/pallas_call | solution.py:654
  69.9 1.4 %copy.16 = bf16[128,128]{1,0:T(8,128)(2,1)} copy(bf16[128,128]{1,0:T(8,128)(2,1)} %layer.1) | data formatting | bytes 65536
